TPU v7x, 128 devices: a whole 4x4x4 slice. The times are simulated.
128 devices in a mesh: fs: 16 (over z, x), tp: 8 (over y, core).
Axes of the slice: x: 4, y: 4, z: 4, core: 2. Of those that a mesh axis runs over, the one named last changes fastest.
Arguments:
- tokens: bfloat16 [16384, 2048], P(('fs', 'tp')), may hold values from -130 to 130
- pool_weight: bfloat16 [4, 512, 512], P(None, 'fs'), may hold values from -0.25 to 0.25
- pool_scale: float32 [2048], replicated, may hold values from 0.5 to 1.5
- gain_mix: float32 [2048], replicated, may hold values from 0.1 to 1.9
- gain_mlp: float32 [2048], replicated, may hold values from 0.1 to 1.9
- w_up: bfloat16 [8192, 2048], P('tp', 'fs'), may hold values from -0.125 to 0.125
- w_down: bfloat16 [8192, 2048], P('tp', 'fs'), may hold values from -0.0625 to 0.0625
- gain_out: float32 [2048], P('tp'), may hold values from 0.1 to 1.9
Outputs:
- result: bfloat16 [16384, 2048], P('fs', 'tp')
All inputs are finite; a program needn't handle non-finite values.
Results may differ from a plain program's by a relative error of at most 0.013.
Values may be sent and summed in bfloat16 or wider, within the bound.
A program may use at most 64 MiB of HBM per device.

v0:
```python
import jax
import jax.numpy as jnp
from jax import lax
from jax.sharding import Mesh
from jax.sharding import PartitionSpec as P

D = 2048
SEQ_LEN = 1024
TP = ("tp_0", "tp_1")
FS_TP = ("fs", "tp_0", "tp_1")


EPS = 1e-06
WINDOWS = (2, 4, 8, 16)


def extended_2(x, sides, width):
    for axis, dim in sides:
        peers, length = (lax.axis_size(axis), x.shape[dim])
        up = [(i, (i + 1) % peers) for i in range(peers - 1)]
        down = [(j, i) for i, j in up]
        last = lax.slice_in_dim(x, length - width, length, axis=dim)
        first = lax.slice_in_dim(x, 0, width, axis=dim)
        before = lax.ppermute(last, axis, up)
        after = lax.ppermute(first, axis, down)
        x = jnp.concatenate([before, x, after], axis=dim)
    return x


def from_everyone(x, axis):
    copies = jnp.broadcast_to(x, (lax.axis_size(axis), *x.shape))
    return lax.all_to_all(copies, axis, split_axis=0, concat_axis=0, tiled=True)


def joined_along(parts, dim):
    parts = jnp.moveaxis(parts, 0, dim)
    dims = parts.shape
    return parts.reshape(*dims[:dim], dims[dim] * dims[dim + 1], *dims[dim + 2 :])


def gather_directly(x, axis, dim):
    parts = from_everyone(x, axis)
    return joined_along(parts, dim)


def whole_of(x, axes, dim):
    far, near = axes
    parts = from_everyone(from_everyone(x, far), near)
    return joined_along(parts.swapaxes(0, 1).reshape(-1, *x.shape), dim)


def in_one_piece(arrays, axis, dim, along):
    both = jnp.concatenate(arrays, axis=along)
    result, at, gathered = (lax.all_gather(both, axis, axis=dim, tiled=True), 0, [])
    for a in arrays:
        gathered.append(lax.slice_in_dim(result, at, at + a.shape[along], axis=along))
        at += a.shape[along]
    return tuple(gathered)


def of_everyone(x, axis):
    return from_everyone(x, axis).sum(axis=0)


def rms_scale(values, gain):
    return values * lax.rsqrt(jnp.mean(values * values, axis=-1, keepdims=True) + EPS) * gain


def local(tokens, pool_weight, pool_scale, gain_mix, gain_mlp, w_up, w_down, gain_out):
    rows = tokens.shape[0]
    width = tokens.shape[1]
    group = width // 4
    offset = lax.axis_index(TP) * rows
    inputs = tokens.astype(jnp.float32)
    normed = rms_scale(inputs, gain_mix).astype(jnp.bfloat16)
    extended = extended_2(normed, ((TP, 0),), 8).astype(jnp.float32)
    line = jnp.arange(rows + 16, dtype=jnp.int32)
    lower_open = offset % SEQ_LEN != 0
    upper_open = (offset + rows) % SEQ_LEN != 0
    keep = jnp.where(line < 8, lower_open, jnp.where(line >= rows + 8, upper_open, True))
    level = extended * keep.astype(jnp.float32)[:, None]
    position = (offset + jnp.arange(rows, dtype=jnp.int32)) % SEQ_LEN
    normed_f32 = normed.astype(jnp.float32)
    full_pool = gather_directly(pool_weight, "fs", 1)
    pieces = []
    for index, reach in enumerate(WINDOWS):
        half = reach // 2
        level = level[:-half] + level[half:]
        start = 8 - half
        window = level[start : start + rows, :group]
        lower = jnp.maximum(position - half, 0)
        upper = jnp.minimum(position + half, SEQ_LEN)
        counts = (upper - lower).astype(jnp.float32)[:, None]
        own = normed_f32[:, index * group : (index + 1) * group]
        pooled = (window / counts - own).astype(jnp.bfloat16)
        pieces.append(jnp.dot(pooled, full_pool[index], preferred_element_type=jnp.float32))
        level = level[:, group:]
    mixed = jnp.concatenate(pieces, axis=1) * pool_scale
    first_sum = (inputs + mixed).astype(jnp.bfloat16)
    inner = rms_scale(first_sum.astype(jnp.float32), gain_mlp).astype(jnp.bfloat16)
    all_inner = whole_of(inner, ("tp_0", "tp_1"), 0)
    contract = (((1,), (1,)), ((), ()))
    up_whole, down_whole = in_one_piece((w_up, w_down), "fs", 1, 0)
    pre = lax.dot_general(all_inner, up_whole, contract, preferred_element_type=jnp.float32)
    hidden = jnp.square(jax.nn.relu(pre)).astype(jnp.bfloat16)
    partial_terms = jnp.dot(hidden, down_whole, preferred_element_type=jnp.float32)
    channel_out = lax.psum_scatter(
        partial_terms.astype(jnp.bfloat16), TP, scatter_dimension=1, tiled=True
    ).astype(jnp.float32)
    first_columns = lax.all_to_all(first_sum, TP, split_axis=1, concat_axis=0, tiled=True)
    second_sum = first_columns.astype(jnp.float32) + channel_out
    squares = of_everyone(jnp.sum(second_sum * second_sum, axis=1), TP)
    scaled = second_sum * lax.rsqrt(squares / D + EPS)[:, None] * gain_out
    return scaled.astype(jnp.bfloat16)


def solution(mesh):
    finer = Mesh(mesh.devices.reshape(mesh.shape["fs"], 4, 2), ("fs", "tp_0", "tp_1"))
    placed = (P(FS_TP, None), P(None, "fs", None), P(), P(), P(), P(TP, "fs"), P(TP, "fs"), P(TP))
    return jax.shard_map(local, mesh=finer, in_specs=placed, out_specs=P("fs", TP), check_vma=False)
```

profile of v0, /device:TPU:1, one launch (start us, length us, event | category | flops | bytes accessed | tf_op | source)
XLA Modules:
  0.0 182.7 jit_solution(17619406736655603106)
XLA Ops:
  6.5 1.9 %pad_maximum_fusion = bf16[2048,128]{1,0:T(8,128)(2,1)} fusion(bf16[1024,128]{1,0:T(8,128)(2,1)} %param.14, bf16[1024,128]{1,0:T(8,128)(2,1)} %param.13), kind=kLoop, calls=%fused_computation.27 | loop fusion | flops 1048576 | bytes 1048576 | tf_op jit(solution)/shard_map/concatenate | solution.py:53
  8.5 1.2 fusion.12
  9.7 1.2 fusion.35
  10.9 4.6 %collective-permute-start = (bf16[8,2048]{1,0:T(8,128)(2,1)S(1)}, bf16[8,2048]{1,0:T(8,128)(2,1)S(1)}, u32[]{:S(2)}, u32[]{:S(2)}) collective-permute-start(bf16[8,2048]{1,0:T(8,128)(2,1)S(1)} %get-tuple-element.15), channel_id=1, source_target_pairs={{0,1},{1,2},{2,3},{3,4},{4,5},{5,6},{6,7},{8,9},{9,10},{10,11},{11... | collective-permute-start | bytes 98312 | tf_op jit(solution)/shard_map/ppermute | solution.py:24
  15.5 1.9 %collective-permute-start.1 = (bf16[8,2048]{1,0:T(8,128)(2,1)S(1)}, bf16[8,2048]{1,0:T(8,128)(2,1)S(1)}, u32[]{:S(2)}, u32[]{:S(2)}) collective-permute-start(bf16[8,2048]{1,0:T(8,128)(2,1)S(1)} %get-tuple-element.16), channel_id=1, source_target_pairs={{1,0},{2,1},{3,2},{4,3},{5,4},{6,5},{7,6},{9,8},{10,9},{11,10},{12... | collective-permute-start | bytes 98312 | tf_op jit(solution)/shard_map/ppermute | solution.py:25
  17.4 1.6 broadcast_in_dim.39
  19.1 7.6 %all-to-all-start = ((bf16[16,4,32,512]{3,2,1,0:T(8,128)(2,1)}), bf16[16,4,32,512]{3,2,1,0:T(8,128)(2,1)S(1)}, u32[]{:S(2)}, u32[]{:S(2)}) async-start(bf16[16,4,32,512]{3,2,1,0:T(8,128)(2,1)} %broadcast_in_dim.39), calls=%async_computation | async-start | bytes 4194304 | tf_op jit(solution)/shard_map/all_to_all | solution.py:32
  28.4 0.9 copy-done
  29.2 0.8 copy-done.3
  30.9 31.1 %all-to-all-done = bf16[16,4,32,512]{3,2,1,0:T(8,128)(2,1)S(1)} async-done(((bf16[16,4,32,512]{3,2,1,0:T(8,128)(2,1)}), bf16[16,4,32,512]{3,2,1,0:T(8,128)(2,1)S(1)}, u32[]{:S(2)}, u32[]{:S(2)}) %all-to-all-start) | async-done | bytes 2097184 | tf_op jit(solution)/shard_map/all_to_all | solution.py:32
  62.1 1.1 copy-done.4
  63.5 1.3 fusion.23
  64.8 1.3 fusion.25
  67.3 27.4 %all_to_all.34 = bf16[4,128,2048]{2,1,0:T(8,128)(2,1)S(1)} all-to-all(bf16[4,128,2048]{2,1,0:T(8,128)(2,1)S(1)} %broadcast_in_dim.40), channel_id=1, replica_groups=mesh['fs'=16,'tp_0'=4,'tp_1'=2] {'tp_0'}, dimensions={0} | all-to-all | bytes 4194304 | tf_op jit(solution)/shard_map/all_to_all | solution.py:32
  95.2 9.4 %all_to_all.35 = bf16[2,4,128,2048]{3,2,1,0:T(8,128)(2,1)S(1)} all-to-all(bf16[2,4,128,2048]{3,2,1,0:T(8,128)(2,1)S(1)} %broadcast_in_dim.41), channel_id=1, replica_groups=mesh['fs'=16,'tp_0'=4,'tp_1'=2] {'tp_1'}, dimensions={0} | all-to-all | bytes 8388608 | tf_op jit(solution)/shard_map/all_to_all | solution.py:32
  104.6 2.3 %copy.16 = bf16[2,4,128,2048]{3,2,0,1:T(8,128)(2,1)} copy(bf16[2,4,128,2048]{3,2,1,0:T(8,128)(2,1)S(1)} %all_to_all.35) | data formatting | bytes 8388608 | tf_op jit(solution)/shard_map/all_to_all | solution.py:32
  106.9 1.8 all-gather.2.cloned.1.call-done
  108.7 8.1 %multiply_convert_fusion = bf16[1024,1024]{1,0:T(8,128)(2,1)S(1)} fusion(bf16[1024,2048]{1,0:T(8,128)(2,1)} %bitcast.28, bf16[2048,2048]{1,0:T(8,128)(2,1)} %all-gather.2.cloned.1.call-done), kind=kOutput, calls=%fused_computation.4 | convolution fusion | flops 4298113024 | bytes 10485760 | tf_op jit(solution)/shard_map/dot_general | solution.py:104
  116.9 6.1 %fusion.4 = bf16[1024,2048]{1,0:T(8,128)(2,1)} fusion(bf16[1024,1024]{1,0:T(8,128)(2,1)S(1)} %multiply_convert_fusion, bf16[2048,2048]{1,0:T(8,128)(2,1)S(1)} %copy-done.11), kind=kOutput, calls=%fused_computation.5 | convolution fusion | flops 4297064448 | bytes 10485760 | tf_op jit(solution)/shard_map/dot_general | solution.py:106
  123.0 16.8 %all_to_all.36 = bf16[128,8,256]{2,0,1:T(8,128)(2,1)S(1)} all-to-all(bf16[128,8,256]{2,0,1:T(8,128)(2,1)S(1)} %bitcast.29), channel_id=1, replica_groups=mesh['fs'=16,'tp_0'=4,'tp_1'=2] {'tp_0','tp_1'}, dimensions={1} | all-to-all | bytes 1048576 | tf_op jit(solution)/shard_map/all_to_all | solution.py:110
  139.8 22.0 %reduce-scatter.2.cloned.1.call-done = bf16[1024,256]{1,0:T(8,128)(2,1)} async-done(((bf16[1024,2048]{1,0:T(8,128)(2,1)}), bf16[1024,256]{1,0:T(8,128)(2,1)}) %reduce-scatter.2.cloned.1.call-update) | async-done | bytes 524304 | tf_op jit(solution)/shard_map/reduce_scatter | solution.py:107
  161.8 1.3 multiply_reduce_fusion
  163.1 10.7 %all_to_all.37 = f32[8,1,1024]{2,1,0:T(1,128)S(1)} all-to-all(f32[8,1,1024]{2,1,0:T(1,128)S(1)} %broadcast_in_dim.42), channel_id=1, replica_groups=mesh['fs'=16,'tp_0'=4,'tp_1'=2] {'tp_0','tp_1'}, dimensions={0} | all-to-all | bytes 65536 | tf_op jit(solution)/shard_map/all_to_all | solution.py:32
  173.8 2.0 %multiply_convert_fusion.1 = bf16[1024,256]{1,0:T(8,128)(2,1)} fusion(bf16[1024,256]{1,0:T(8,128)(2,1)} %reduce-scatter.2.cloned.1.call-done, bf16[128,8,256]{2,0,1:T(8,128)(2,1)S(1)} %all_to_all.36, f32[256]{0:T(256)S(1)} %copy-done.10, f32[1024]{0:T(1024)S(1)} %add_rsqrt_fusion), kind=kLoop, calls=%fused_computation.22 | loop fusion | flops 1572864 | bytes 1577984 | tf_op jit(solution)/shard_map/convert_element_type | solution.py:114
  (57 shorter events, 4.6 us)
Async XLA Ops:
  6.5 3.2 %copy-start.1 = (bf16[128,2048]{1,0:T(8,128)(2,1)S(1)}, bf16[128,2048]{1,0:T(8,128)(2,1)}, u32[]{:S(2)}) copy-start(bf16[128,2048]{1,0:T(8,128)(2,1)} %param.8) | copy-start | bytes 1572868
  6.5 3.2 %copy-start.7 = (f32[2048]{0:T(1024)S(1)}, f32[2048]{0:T(1024)}, u32[]{:S(2)}) copy-start(f32[2048]{0:T(1024)} %param.11) | copy-start | bytes 24580
  6.5 10.9 %copy-start.6 = (bf16[4,32,512]{2,1,0:T(8,128)(2,1)S(1)}, bf16[4,32,512]{2,1,0:T(8,128)(2,1)}, u32[]{:S(2)}) copy-start(bf16[4,32,512]{2,1,0:T(8,128)(2,1)} %param.9) | copy-start | bytes 393220
  6.5 102.2 %all-gather.2.cloned.1.call-start = ((), (), s32[]{:S(2)}) async-start(), calls=%async_computation.6 | async-start | bytes 8912896 | tf_op jit(solution)/shard_map/all_gather | solution.py:54
  10.9 16.9 %collective-permute-start = (bf16[8,2048]{1,0:T(8,128)(2,1)S(1)}, bf16[8,2048]{1,0:T(8,128)(2,1)S(1)}, u32[]{:S(2)}, u32[]{:S(2)}) collective-permute-start(bf16[8,2048]{1,0:T(8,128)(2,1)S(1)} %get-tuple-element.15), channel_id=1, source_target_pairs={{0,1},{1,2},{2,3},{3,4},{4,5},{5,6},{6,7},{8,9},{9,10},{10,11},{11... | collective-permute-start | bytes 98312 | tf_op jit(solution)/shard_map/ppermute | solution.py:24
  15.5 12.3 %collective-permute-start.1 = (bf16[8,2048]{1,0:T(8,128)(2,1)S(1)}, bf16[8,2048]{1,0:T(8,128)(2,1)S(1)}, u32[]{:S(2)}, u32[]{:S(2)}) collective-permute-start(bf16[8,2048]{1,0:T(8,128)(2,1)S(1)} %get-tuple-element.16), channel_id=1, source_target_pairs={{1,0},{2,1},{3,2},{4,3},{5,4},{6,5},{7,6},{9,8},{10,9},{11,10},{12... | collective-permute-start | bytes 98312 | tf_op jit(solution)/shard_map/ppermute | solution.py:25
  19.1 42.9 %all-to-all-start = ((bf16[16,4,32,512]{3,2,1,0:T(8,128)(2,1)}), bf16[16,4,32,512]{3,2,1,0:T(8,128)(2,1)S(1)}, u32[]{:S(2)}, u32[]{:S(2)}) async-start(bf16[16,4,32,512]{3,2,1,0:T(8,128)(2,1)} %broadcast_in_dim.39), calls=%async_computation | async-start | bytes 4194304 | tf_op jit(solution)/shard_map/all_to_all | solution.py:32
  26.7 135.1 %reduce-scatter.2.cloned.1.call-start = ((), (), s32[]{:S(2)}) async-start(), calls=%async_computation.7 | async-start | bytes 4718592 | tf_op jit(solution)/shard_map/reduce_scatter | solution.py:107
  28.3 0.9 copy-start
  29.2 0.8 copy-start.3
  62.0 1.2 copy-start.4
  62.0 1.2 copy-start.15
  62.0 1.5 copy-start.14
  62.1 2.7 %copy-start.13 = (f32[128]{0:T(128)S(1)}, f32[128]{0:T(128)}, u32[]{:S(2)}) copy-start(f32[128]{0:T(128)} %get-tuple-element.18) | copy-start | bytes 1540
  63.5 2.7 %copy-start.5 = (f32[129,512]{1,0:T(8,128)S(1)}, f32[129,512]{1,0:T(8,128)}, u32[]{:S(2)}) copy-start(f32[129,512]{1,0:T(8,128)} %get-tuple-element.14) | copy-start | bytes 792580
  63.5 2.7 %copy-start.12 = (f32[128]{0:T(128)S(1)}, f32[128]{0:T(128)}, u32[]{:S(2)}) copy-start(f32[128]{0:T(128)} %get-tuple-element.17) | copy-start | bytes 1540
  64.8 1.7 copy-start.2
  64.8 1.7 copy-start.8
  66.1 0.7 copy-start.9
  108.7 8.1 %copy-start.11 = (bf16[2048,2048]{1,0:T(8,128)(2,1)S(1)}, bf16[2048,2048]{1,0:T(8,128)(2,1)}, u32[]{:S(2)}) copy-start(bf16[2048,2048]{1,0:T(8,128)(2,1)} %all-gather.2.cloned.1.call-done) | copy-start | bytes 25165828
  123.0 50.9 %copy-start.10 = (f32[256]{0:T(256)S(1)}, f32[256]{0:T(256)}, u32[]{:S(2)}) copy-start(f32[256]{0:T(256)} %param.15) | copy-start | bytes 3076
Sparse Core Ops, SparseCore 0:
  9.4 99.2 all-gather.1
  123.1 38.6 reduce-scatter.1
where the time goes:
time: 183 us
  blocking collectives  64.3 us (35%)
  waiting for transfers between devices  54.9 us (30%)
  matrix products  17.4 us (10%)
  starting transfers between devices  14.1 us (8%)
  between operations  13.7 us (7%)
  other arithmetic  9.75 us (5%)
  local copies, waits for them, and re-layouts  8.53 us (5%)
    all_to_all x3, blocking collectives, from_everyone(): return lax.all_to_all(copies, axis, split_axis=0, concat_axis=0, tiled=True)  47.5 us
    all_to_all x1, waiting for transfers between devices, from_everyone(): return lax.all_to_all(copies, axis, split_axis=0, concat_axis=0, tiled=True)  31.1 us
    reduce_scatter x1, waiting for transfers between devices, local(): lax.psum_scatter(partial_terms.astype(jnp.bfloat16), TP, scatter_dimensio...  22 us
    all_to_all x1, blocking collectives, local(): lax.all_to_all(first_sum, TP, split_axis=1, concat_axis=0, tiled=True)  16.8 us
    dot_general x1, matrix products, local(): lax.dot_general(all_inner, up_whole, contract, preferred_element_type=jnp...  8.13 us
    all_to_all x1, starting transfers between devices, from_everyone(): return lax.all_to_all(copies, axis, split_axis=0, concat_axis=0, tiled=True)  7.6 us
    dot_general x1, matrix products, local(): jnp.dot(hidden, down_whole, preferred_element_type=jnp.float32)  6.07 us
    ppermute x1, starting transfers between devices, extended_2(): before = lax.ppermute(last, axis, up)  4.57 us
  transfers between devices with their start and end apart: 5, of which 3 were waited for; matrix products, arithmetic and copies ran while one was open for 7% of the time, Pallas kernels for 0%

commit v1 on v0

v1 whole, which is shorter than its diff:
```python
import functools

import jax
import jax.numpy as jnp
from jax import lax
from jax.experimental import pallas as pl
from jax.experimental.pallas import tpu as pltpu
from jax.sharding import PartitionSpec as P

D = 2048
SEQ = 1024
EPS = 1e-06
F32 = jnp.float32
BF16 = jnp.bfloat16
MESH = pl.DeviceIdType.MESH
CH = 256
NCH = SEQ // CH
HALF = SEQ // 2


def kernel(tok, pw, up, dn, pscale, gmix, gmlp, gout, out,
           tokv, X, NB, R, RT, PB, UB, DB, PL2, G, SQ, SQ2, H, PART, SO, SB, RH, RY, ACC,
           lsem, as_, ar, rs_, rr, ps, pr, us, ur, ds_, dr, xs, xr, gs, gr, ss, sr, ts, tr, cs, cr, ys, yr):
    f = lax.axis_index("fs")
    t = lax.axis_index("tp")
    z, x = f // 4, f % 4
    y, c = t // 2, t % 2

    def fa(d):
        return (1 - c) * (4 * z + (x + d) % 4) + c * (4 * ((z + d) % 4) + x)

    def fb(d):
        return (1 - c) * (4 * ((z + d) % 4) + x) + c * (4 * z + (x + d) % 4)

    pa = (1 - c) * x + c * z
    pb = (1 - c) * z + c * x

    def slot(i, j):
        return 4 * ((pb + j) % 4) + (pa + i) % 4

    def slot_of(g):
        return (1 - c) * g + c * (4 * (g % 4) + g // 4)

    def remote(src, dst, ssem, rsem, fs, tp):
        return pltpu.make_async_remote_copy(
            src_ref=src, dst_ref=dst, send_sem=ssem, recv_sem=rsem,
            device_id={"fs": fs, "tp": tp}, device_id_type=MESH)

    sib = 2 * y + 1 - c
    yp = 2 * ((y + 1) % 4) + c
    ym = 2 * ((y + 3) % 4) + c
    own = slot(0, 0)

    c_tok = pltpu.make_async_copy(tok, tokv, lsem.at[0])
    c_x = pltpu.make_async_copy(
        tok.at[:, pl.ds(pl.multiple_of(256 * t, 256), 256)],
        X.at[pl.ds(pl.multiple_of(128 * t, 128), 128)], lsem.at[1])
    c_u = pltpu.make_async_copy(up, UB.at[own], lsem.at[2])
    c_d = pltpu.make_async_copy(dn, DB.at[own], lsem.at[3])
    c_p = pltpu.make_async_copy(
        pw.at[y, :, pl.ds(pl.multiple_of(256 * c, 256), 256)], PB.at[own], lsem.at[4])
    for cp in (c_tok, c_p, c_u, c_x, c_d):
        cp.start()
    barrier = pltpu.get_barrier_semaphore()
    for e in (1, 2, 3):
        pl.semaphore_signal(barrier, inc=1, device_id={"fs": fa(e), "tp": t}, device_id_type=MESH)
        pl.semaphore_signal(barrier, inc=1, device_id={"fs": fb(e), "tp": t}, device_id_type=MESH)
    for e in range(1, 8):
        pl.semaphore_signal(barrier, inc=1, device_id={"fs": f, "tp": (t + e) % 8}, device_id_type=MESH)
    c_tok.wait()
    c_p.wait()
    c_u.wait()
    pl.semaphore_wait(barrier, 13)

    def a2a(e):
        p = (t + e) % 8
        return remote(tokv.at[:, pl.ds(pl.multiple_of(256 * p, 256), 256)],
                      X.at[pl.ds(pl.multiple_of(128 * t, 128), 128)], as_.at[e - 1], ar.at[e - 1], f, p)

    for e in (4, 3, 5, 2, 6, 1, 7):
        a2a(e).start()

    def p_a(e):
        return remote(PB.at[own], PB.at[own], ps.at[e - 1], pr.at[e - 1], fa(e), t)

    def p_b(e):
        line = PB.at[pl.ds(4 * pb, 4)]
        return remote(line, line, ps.at[2 + e], pr.at[2 + e], fb(e), t)

    for e in (1, 3, 2):
        p_a(e).start()

    hrows = (pl.ds(0, HALF), pl.ds(HALF, HALF))
    offs = (0, 3, 1, 2)

    def w_a0(W, s, r, d):
        ref = W.at[own]
        return remote(ref, ref, s.at[d], r.at[d], fa(1 if d == 0 else 3), t)

    def w_a2(W, s, r, d):
        ref = W.at[slot(3 if d == 0 else 1, 0), hrows[d]]
        return remote(ref, ref, s.at[2 + d], r.at[2 + d], fa(1 if d == 0 else 3), t)

    def w_b(W, s, r, n, d):
        ref = W.at[slot(offs[n], 0)]
        return remote(ref, ref, s.at[4 + 2 * n + d], r.at[4 + 2 * n + d], fb(1 if d == 0 else 3), t)

    def w_b2(W, s, r, n, d):
        ref = W.at[slot(offs[n], 3 if d == 0 else 1), hrows[d]]
        return remote(ref, ref, s.at[12 + 2 * n + d], r.at[12 + 2 * n + d], fb(1 if d == 0 else 3), t)

    def pump_a0(W, s, r):
        for d in (0, 1):
            w_a0(W, s, r, d).start()

    def pump_b(W, s, r, n):
        for d in (0, 1):
            w_b(W, s, r, n, d).start()

    def pump_a1(W, s, r):
        for d in (0, 1):
            w_a0(W, s, r, d).wait_recv()
        for d in (0, 1):
            w_a2(W, s, r, d).start()
        pump_b(W, s, r, 1)
        pump_b(W, s, r, 2)

    def pump_a2(W, s, r):
        for d in (0, 1):
            w_a2(W, s, r, d).wait_recv()
        pump_b(W, s, r, 3)

    def pump_b1(W, s, r, n):
        for d in (0, 1):
            w_b(W, s, r, n, d).wait_recv()
            w_b2(W, s, r, n, d).start()

    def pump_b2(W, s, r, n):
        for d in (0, 1):
            w_b2(W, s, r, n, d).wait_recv()

    U = (UB, us, ur)
    V = (DB, ds_, dr)
    pump_a0(*U)

    ri = lax.broadcasted_iota(jnp.int32, (128, 128), 0)
    ci = lax.broadcasted_iota(jnp.int32, (128, 128), 1)
    eye = (ri == ci).astype(F32)

    def to_lanes(col):
        return jnp.sum(col * eye, axis=0, keepdims=True)

    def to_column(lanes):
        return jnp.sum(lanes * eye, axis=1, keepdims=True)

    v = tokv[...].astype(F32)
    r1 = lax.rsqrt(jnp.sum(v * v, axis=1, keepdims=True) / D + EPS)
    R[t] = jnp.broadcast_to(to_lanes(r1), (8, 128))

    def r_x(e):
        return remote(R.at[t], R.at[t], rs_.at[e - 1], rr.at[e - 1], f, (t + e) % 8)

    for e in range(1, 8):
        r_x(e).start()

    for e in (1, 3, 2):
        p_a(e).wait_recv()
    for e in (1, 3, 2):
        p_b(e).start()
    pump_b(*U, 0)
    pump_a1(*U)

    def row_of(ref):
        return jnp.concatenate([ref[pl.ds(2 * t, 1), :], ref[pl.ds(2 * t + 1, 1), :]], axis=1)

    gm = row_of(gmix)
    NB[pl.ds(0, 16), :] = jnp.zeros((16, 256), BF16)
    NB[pl.ds(16 + SEQ, 16), :] = jnp.zeros((16, 256), BF16)
    c_x.wait()
    c_d.wait()
    for e in range(1, 8):
        a2a(e).wait_recv()
        r_x(e).wait_recv()
    for i in range(8):
        rc = to_column(R[i, 0:1, :])
        xv = X[pl.ds(128 * i, 128), :].astype(F32)
        NB[pl.ds(16 + 128 * i, 128), :] = (xv * rc * gm).astype(BF16)

    reach = 1 + (y >= 1).astype(jnp.int32) + 2 * (y >= 2).astype(jnp.int32) + 4 * (y >= 3).astype(jnp.int32)
    bi = lax.broadcasted_iota(jnp.int32, (128, 160), 0)
    bj = lax.broadcasted_iota(jnp.int32, (128, 160), 1)
    delta = bj - 16 - bi
    band = jnp.where((delta >= -reach) & (delta < reach), 1.0, 0.0).astype(BF16)

    def pl_x(q):
        ref = PL2.at[c, pl.ds(CH * q, CH)]
        return remote(ref, ref, xs.at[q], xr.at[q], f, sib)

    for i in range(8):
        sums = jnp.dot(band, NB[pl.ds(128 * i, 160), :], preferred_element_type=F32)
        pos = 128 * i + lax.broadcasted_iota(jnp.int32, (128, 256), 0)
        count = jnp.minimum(pos + reach, SEQ) - jnp.maximum(pos - reach, 0)
        mine = NB[pl.ds(16 + 128 * i, 128), :].astype(F32)
        PL2[c, pl.ds(128 * i, 128), :] = (sums / count.astype(F32) - mine).astype(BF16)
        if i % 2 == 1:
            pl_x(i // 2).start()

    pump_a2(*U)
    for e in (1, 3, 2):
        p_b(e).wait_recv()

    psc = row_of(pscale)
    gml = row_of(gmlp)

    def g_ref(owner, q):
        return G.at[owner, pl.ds(CH * q, CH)]

    def g_y(q, d):
        return remote(g_ref(t, q), g_ref(t, q), gs.at[2 * q + d], gr.at[2 * q + d], f, yp if d == 0 else ym)

    def g_sib(k, q):
        owner = (t + (0, 6, 2, 4)[k]) % 8
        return remote(g_ref(owner, q), g_ref(owner, q), gs.at[8 + 4 * k + q], gr.at[8 + 4 * k + q], f, sib)

    def g_fwd(q):
        owner = ym if q < 2 else yp
        return remote(g_ref(owner, q), g_ref(owner, q), gs.at[24 + q], gr.at[24 + q], f, yp if q < 2 else ym)

    pk = [jnp.concatenate([PB[slot_of(8 * k + i)] for i in range(8)], axis=0) for k in (0, 1)]
    for q in range(NCH):
        pl_x(q).wait_recv()
        rows = pl.ds(CH * q, CH)
        mixed = (jnp.dot(PL2[0, rows, :], pk[0], preferred_element_type=F32)
                 + jnp.dot(PL2[1, rows, :], pk[1], preferred_element_type=F32)) * psc
        first = (X[rows, :].astype(F32) + mixed).astype(BF16).astype(F32)
        G[t, rows, :] = (first * gml).astype(BF16)
        for d in (0, 1):
            g_y(q, d).start()
        g_sib(0, q).start()
        ACC[0, rows, :] = first[:, :128]
        ACC[1, rows, :] = first[:, 128:]
        sq = jnp.sum(first * first, axis=1, keepdims=True)
        for h in (0, 1):
            SQ[t, pl.ds(2 * q + h, 1), :] = to_lanes(sq[128 * h:128 * h + 128])

    def sq_x(e):
        return remote(SQ.at[t], SQ.at[t], ss.at[e - 1], sr.at[e - 1], f, (t + e) % 8)

    for e in range(1, 8):
        sq_x(e).start()

    def g_pump(q):
        g_y(q, 0).wait_recv()
        if q < 2:
            g_fwd(q).start()
        g_sib(1, q).start()
        g_y(q, 1).wait_recv()
        if q >= 2:
            g_fwd(q).start()
        g_sib(2, q).start()

    def g_pump2(q):
        g_fwd(q).wait_recv()
        g_sib(3, q).start()

    pump_b1(*U, 0)
    g_pump(0)
    pump_b1(*U, 1)
    g_pump(1)
    pump_b1(*U, 2)
    pump_b1(*U, 3)
    pump_a0(*V)
    pump_b(*V, 0)
    g_pump(2)
    g_pump2(0)
    g_pump(3)
    g_pump2(1)
    g_pump2(2)
    for n in range(4):
        pump_b2(*U, n)
    pump_a1(*V)
    g_pump2(3)

    for e in range(1, 8):
        sq_x(e).wait_recv()
    total = SQ[0]
    for i in range(1, 8):
        total = total + SQ[i]
    RT[...] = lax.rsqrt(total / D + EPS)
    for k in range(4):
        for q in range(NCH):
            g_sib(k, q).wait_recv()

    def up_rows(q, carry):
        base = pl.multiple_of(CH * q, CH)
        rows = pl.ds(base, CH)
        rc = jnp.concatenate([to_column(RT[pl.ds(2 * q + h, 1), :]) for h in (0, 1)], axis=0)
        lhs = jnp.concatenate([G[i, rows, :] for i in range(8)], axis=1)

        def cols(h, carry):
            hs = pl.ds(pl.multiple_of(256 * h, 256), 256)
            rhs = jnp.concatenate([UB[slot_of(g), hs, :] for g in range(16)], axis=1)
            pre = lax.dot_general(lhs, rhs, (((1,), (1,)), ((), ())), preferred_element_type=F32)
            act = jnp.maximum(pre * rc, 0.0)
            H[rows, hs] = (act * act).astype(BF16)
            return carry

        return lax.fori_loop(0, 4, cols, carry)

    lax.fori_loop(0, NCH, up_rows, 0)
    pump_a2(*V)
    for n in range(4):
        pump_b1(*V, n)
    for n in range(4):
        pump_b2(*V, n)

    def so(k, d):
        return SO.at[k, d]

    def c_x2(k, d):
        return remote(SO.at[k, d], SB.at[k, d], cs.at[4 * k + d], cr.at[4 * k + d], f, sib)

    def y_half(k, d):
        return remote(SO.at[k, 2, hrows[d]], RH.at[k, d], ys.at[4 * k + d], yr.at[4 * k + d], f, yp if d == 0 else ym)

    def y_full(k, d):
        return remote(SO.at[k, 1 if d == 0 else 3], RY.at[k, d], ys.at[4 * k + 2 + d], yr.at[4 * k + 2 + d], f,
                      yp if d == 0 else ym)

    for k in range(4):
        xk = (x + offs[k]) % 4
        owner = xk // 2 == c
        helper = xk // 2 != c
        half = xk % 2

        def down(q, carry):
            rows = pl.ds(pl.multiple_of(CH * q, CH), CH)
            rhs = jnp.concatenate([DB[slot_of(4 * ((y + d) % 4) + xk)] for d in range(4)], axis=1)
            PART[rows, :] = jnp.dot(H[rows, :], rhs, preferred_element_type=F32)
            return carry

        lax.fori_loop(0, NCH, down, 0)

        @pl.when(helper)
        def _():
            for d in (2, 1, 3, 0):
                SO[k, d] = PART[:, 128 * d:128 * d + 128].astype(BF16)
                c_x2(k, d).start()
            for d in (2, 1, 3, 0):
                c_x2(k, d).wait_send()

        @pl.when(owner)
        def _():
            c_x2(k, 2).wait_recv()
            SO[k, 2] = (PART[:, 256:384] + SB[k, 2].astype(F32)).astype(BF16)
            y_half(k, 0).start()
            y_half(k, 1).start()
            c_x2(k, 1).wait_recv()
            c_x2(k, 3).wait_recv()
            y_half(k, 0).wait_recv()
            SO[k, 1, hrows[0]] = (PART[hrows[0], 128:256] + SB[k, 1, hrows[0]].astype(F32)
                                  + RH[k, 0].astype(F32)).astype(BF16)
            SO[k, 1, hrows[1]] = (PART[hrows[1], 128:256] + SB[k, 1, hrows[1]].astype(F32)).astype(BF16)
            y_full(k, 0).start()
            y_half(k, 1).wait_recv()
            SO[k, 3, hrows[0]] = (PART[hrows[0], 384:512] + SB[k, 3, hrows[0]].astype(F32)).astype(BF16)
            SO[k, 3, hrows[1]] = (PART[hrows[1], 384:512] + SB[k, 3, hrows[1]].astype(F32)
                                  + RH[k, 1].astype(F32)).astype(BF16)
            y_full(k, 1).start()
            c_x2(k, 0).wait_recv()
            ACC[half] = ACC[half] + PART[:, 0:128] + SB[k, 0].astype(F32)

    for k in range(4):
        xk = (x + offs[k]) % 4
        owner = xk // 2 == c
        half = xk % 2

        @pl.when(owner)
        def _():
            y_full(k, 0).wait_recv()
            y_full(k, 1).wait_recv()
            ACC[half] = ACC[half] + RY[k, 0].astype(F32) + RY[k, 1].astype(F32)
            for d in (0, 1):
                y_half(k, d).wait_send()
                y_full(k, d).wait_send()

    for i in range(8):
        rows = pl.ds(128 * i, 128)
        a0, a1 = ACC[0, rows, :], ACC[1, rows, :]
        SQ2[t, pl.ds(i, 1), :] = to_lanes(jnp.sum(a0 * a0 + a1 * a1, axis=1, keepdims=True))

    def t_x(e):
        return remote(SQ2.at[t], SQ2.at[t], ts.at[e - 1], tr.at[e - 1], f, (t + e) % 8)

    for e in range(1, 8):
        t_x(e).start()
    for e in range(1, 8):
        t_x(e).wait_recv()
    total = SQ2[0]
    for i in range(1, 8):
        total = total + SQ2[i]
    rl = lax.rsqrt(total / D + EPS)
    for i in range(8):
        rows = pl.ds(128 * i, 128)
        rc = to_column(rl[i:i + 1, :])
        for h in (0, 1):
            out[rows, 128 * h:128 * h + 128] = (ACC[h, rows, :] * rc * gout[h:h + 1, :]).astype(BF16)

    for e in range(1, 8):
        a2a(e).wait_send()
        r_x(e).wait_send()
        sq_x(e).wait_send()
        t_x(e).wait_send()
    for e in (1, 2, 3):
        p_a(e).wait_send()
        p_b(e).wait_send()
    for W in (U, V):
        for d in (0, 1):
            w_a0(*W, d).wait_send()
            w_a2(*W, d).wait_send()
            for n in range(4):
                w_b(*W, n, d).wait_send()
                w_b2(*W, n, d).wait_send()
    for q in range(NCH):
        pl_x(q).wait_send()
        g_y(q, 0).wait_send()
        g_y(q, 1).wait_send()
        g_fwd(q).wait_send()
        for k in range(4):
            g_sib(k, q).wait_send()


def local(tokens, pool_weight, pool_scale, gain_mix, gain_mlp, w_up, w_down, gain_out):
    dma = pltpu.SemaphoreType.DMA
    hbm = pl.BlockSpec(memory_space=pl.ANY)
    vmem = pl.BlockSpec(memory_space=pltpu.VMEM)
    return pl.pallas_call(
        kernel,
        out_shape=jax.ShapeDtypeStruct((SEQ, 256), BF16),
        in_specs=[hbm] * 4 + [vmem] * 4,
        out_specs=vmem,
        scratch_shapes=[
            pltpu.VMEM((128, D), BF16),
            pltpu.VMEM((SEQ, 256), BF16),
            pltpu.VMEM((SEQ + 32, 256), BF16),
            pltpu.VMEM((8, 8, 128), F32),
            pltpu.VMEM((8, 128), F32),
            pltpu.VMEM((16, 32, 256), BF16),
            pltpu.VMEM((16, 1024, 128), BF16),
            pltpu.VMEM((16, 1024, 128), BF16),
            pltpu.VMEM((2, SEQ, 256), BF16),
            pltpu.VMEM((8, SEQ, 256), BF16),
            pltpu.VMEM((8, 8, 128), F32),
            pltpu.VMEM((8, 8, 128), F32),
            pltpu.VMEM((SEQ, 1024), BF16),
            pltpu.VMEM((SEQ, 512), F32),
            pltpu.VMEM((4, 4, SEQ, 128), BF16),
            pltpu.VMEM((4, 4, SEQ, 128), BF16),
            pltpu.VMEM((4, 2, HALF, 128), BF16),
            pltpu.VMEM((4, 2, SEQ, 128), BF16),
            pltpu.VMEM((2, SEQ, 128), F32),
            dma((5,)),
            dma((7,)), dma((7,)),
            dma((7,)), dma((7,)),
            dma((6,)), dma((6,)),
            dma((20,)), dma((20,)),
            dma((20,)), dma((20,)),
            dma((4,)), dma((4,)),
            dma((28,)), dma((28,)),
            dma((7,)), dma((7,)),
            dma((7,)), dma((7,)),
            dma((16,)), dma((16,)),
            dma((16,)), dma((16,)),
        ],
        compiler_params=pltpu.CompilerParams(
            collective_id=0, has_side_effects=True, vmem_limit_bytes=60 * 1024 * 1024),
        name="mixers",
    )(tokens, pool_weight, w_up, w_down, pool_scale.reshape(16, 128), gain_mix.reshape(16, 128),
      gain_mlp.reshape(16, 128), gain_out.reshape(2, 128))


def solution(mesh):
    placed = (P(("fs", "tp"), None), P(None, "fs", None), P(), P(), P(), P("tp", "fs"), P("tp", "fs"), P("tp"))
    return jax.shard_map(local, mesh=mesh, in_specs=placed, out_specs=P("fs", "tp"), check_vma=False)
```

time: 183 us -> 107 us (0.58)
  Pallas kernels: 0 us -> 105 us
  blocking collectives: 64.3 us -> 0 us
  waiting for transfers between devices: 54.9 us -> 0 us
  matrix products: 17.4 us -> 0 us
  starting transfers between devices: 14.1 us -> 0 us
  between operations: 13.7 us -> 0.01 us
  other arithmetic: 9.75 us -> 0 us
  local copies, waits for them, and re-layouts: 8.53 us -> 1.87 us
    pallas_call x0 -> x1, Pallas kernels: none -> 105 us  [local(): pl.pallas_call(kernel, out_shape=jax.ShapeDtypeStruct((SEQ, 256), BF16),...]
    all_to_all x4 -> x0, blocking collectives: 64.3 us -> none  [the longest x3 47.5 us: from_everyone(): return lax.all_to_all(copies, axis, split_axis=0, concat_axis=0, tiled=True)]
    all_to_all x1 -> x0, waiting for transfers between devices: 31.1 us -> none  [from_everyone(): return lax.all_to_all(copies, axis, split_axis=0, concat_axis=0, tiled=True)]
    reduce_scatter x1 -> x0, waiting for transfers between devices: 22 us -> none  [local(): lax.psum_scatter(partial_terms.astype(jnp.bfloat16), TP, scatter_dimensio...]
    dot_general x6 -> x0, matrix products: 17.4 us -> none  [the longest x1 8.13 us: local(): lax.dot_general(all_inner, up_whole, contract, preferred_element_type=jnp...]
    all_to_all x1 -> x0, starting transfers between devices: 7.6 us -> none  [from_everyone(): return lax.all_to_all(copies, axis, split_axis=0, concat_axis=0, tiled=True)]
    ppermute x2 -> x0, starting transfers between devices: 6.49 us -> none  [the longest x1 4.57 us: extended_2(): before = lax.ppermute(last, axis, up)]
    convert_element_type x6 -> x0, other arithmetic: 4.48 us -> none  [the longest x1 2.05 us: local(): return scaled.astype(jnp.bfloat16)]
  transfers between devices with their start and end apart: 5 -> 0, of which waited for: 3 -> 0; matrix products, arithmetic and copies ran while one was open for 7% -> 0% of each run, Pallas kernels for 0% -> 0%
where the time goes in v1:
time: 107 us
  Pallas kernels  105 us (98%)
  local copies, waits for them, and re-layouts  1.87 us (2%)
    pallas_call x1, Pallas kernels, local(): pl.pallas_call(kernel, out_shape=jax.ShapeDtypeStruct((SEQ, 256), BF16),...  105 us

profile of v1, /device:TPU:1, one launch (start us, length us, event | category | flops | bytes accessed | tf_op | source)
XLA Modules:
  0.0 107.0 jit_solution(11817412453158130321)
XLA Ops:
  0.0 105.1 %mixers.1 = bf16[1024,256]{1,0:T(8,128)(2,1)} custom-call(bf16[128,2048]{1,0:T(8,128)(2,1)} %tok.1, bf16[4,32,512]{2,1,0:T(8,128)(2,1)} %pw.1, bf16[1024,128]{1,0:T(8,128)(2,1)} %up.1, bf16[1024,128]{1,0:T(8,128)(2,1)} %dn.1, f32[16,128]{1,0:T(8,128)} %bitcast.4, f32[16,128]{1,0:T(8,128)} %bitcast.5, f32[16,128]{1,0:T(8,128)} %bitcast.6, f32[2,128]{1,0:T(2,128)} %bitcast.7), custom_call_target="tpu_custom_call" | custom-call | tf_op jit(solution)/shard_map/mixers/pallas_call | solution.py:437
  105.1 1.9 %copy.10 = bf16[1024,256]{1,0:T(8,128)(2,1)} copy(bf16[1024,256]{1,0:T(8,128)(2,1)} %mixers.1) | data formatting | bytes 1048576

commit v2 on v1

--- a/solution.py
+++ b/solution.py
@@ -18,9 +18,21 @@
 HALF = SEQ // 2
 
 
+class Phases:
+    now = None
+
+    def __call__(self, name):
+        if self.now is not None:
+            self.now.__exit__(None, None, None)
+        self.now = jax.named_scope(name) if name else None
+        if name:
+            self.now.__enter__()
+
+
 def kernel(tok, pw, up, dn, pscale, gmix, gmlp, gout, out,
-           tokv, X, NB, R, RT, PB, UB, DB, PL2, G, SQ, SQ2, H, PART, SO, SB, RH, RY, ACC,
+           tokv, RL, X, NB, R, RT, PB, UB, DB, PL2, G, SQ, SQ2, H, PART, SO, SB, RH, RY, ACC,
            lsem, as_, ar, rs_, rr, ps, pr, us, ur, ds_, dr, xs, xr, gs, gr, ss, sr, ts, tr, cs, cr, ys, yr):
+    ph = Phases()
     f = lax.axis_index("fs")
     t = lax.axis_index("tp")
     z, x = f // 4, f % 4
@@ -51,6 +63,7 @@
     ym = 2 * ((y + 3) % 4) + c
     own = slot(0, 0)
 
+    ph("a_entry")
     c_tok = pltpu.make_async_copy(tok, tokv, lsem.at[0])
     c_x = pltpu.make_async_copy(
         tok.at[:, pl.ds(pl.multiple_of(256 * t, 256), 256)],
@@ -62,23 +75,69 @@
     for cp in (c_tok, c_p, c_u, c_x, c_d):
         cp.start()
     barrier = pltpu.get_barrier_semaphore()
+    for e in range(1, 8):
+        pl.semaphore_signal(barrier, inc=1, device_id={"fs": f, "tp": (t + e) % 8}, device_id_type=MESH)
     for e in (1, 2, 3):
         pl.semaphore_signal(barrier, inc=1, device_id={"fs": fa(e), "tp": t}, device_id_type=MESH)
         pl.semaphore_signal(barrier, inc=1, device_id={"fs": fb(e), "tp": t}, device_id_type=MESH)
-    for e in range(1, 8):
-        pl.semaphore_signal(barrier, inc=1, device_id={"fs": f, "tp": (t + e) % 8}, device_id_type=MESH)
+
+    ri = lax.broadcasted_iota(jnp.int32, (128, 128), 0)
+    ci = lax.broadcasted_iota(jnp.int32, (128, 128), 1)
+    eye = (ri == ci).astype(F32)
+
+    def to_lanes(col):
+        return jnp.sum(col * eye, axis=0, keepdims=True)
+
+    def to_column(lanes):
+        return jnp.sum(lanes * eye, axis=1, keepdims=True)
+
     c_tok.wait()
+    v = tokv[...].astype(F32)
+    r1 = lax.rsqrt(jnp.sum(v * v, axis=1, keepdims=True) / D + EPS)
+    R[t] = jnp.broadcast_to(to_lanes(r1), (8, 128))
     c_p.wait()
     c_u.wait()
+    c_d.wait()
     pl.semaphore_wait(barrier, 13)
 
-    def a2a(e):
-        p = (t + e) % 8
-        return remote(tokv.at[:, pl.ds(pl.multiple_of(256 * p, 256), 256)],
-                      X.at[pl.ds(pl.multiple_of(128 * t, 128), 128)], as_.at[e - 1], ar.at[e - 1], f, p)
-
-    for e in (4, 3, 5, 2, 6, 1, 7):
-        a2a(e).start()
+    ph("b_start")
+    via = (y + 1 + 2 * c) % 4
+
+    def rows_of(o):
+        return pl.ds(pl.multiple_of(128 * o, 128), 128)
+
+    def near(n):
+        p = (2 * ((y + (1 if n < 2 else 3)) % 4) + n % 2) if n < 4 else sib
+        return remote(tokv.at[:, pl.ds(pl.multiple_of(256 * p, 256), 256)], X.at[rows_of(t)], as_.at[n], ar_of(n), f, p)
+
+    def ar_of(n):
+        return ar.at[(2 if n < 2 else 0) + c] if n < 4 else ar.at[4]
+
+    def near_in(n):
+        o = (2 * ((y + (1 if n < 2 else 3)) % 4) + n % 2) if n < 4 else sib
+        return pltpu.make_async_copy(X.at[rows_of(o)], X.at[rows_of(o)], ar.at[n])
+
+    def relay_out():
+        return remote(tokv.at[:, pl.ds(pl.multiple_of(512 * ((y + 2) % 4), 512), 512)], RL,
+                      as_.at[5], ar.at[5], f, 2 * via + c)
+
+    def relay_on(k):
+        o = 2 * ((y + 3 + 2 * c) % 4) + c
+        return remote(RL.at[:, pl.ds(256 * k, 256)], X.at[rows_of(o)], as_.at[6 + k], ar.at[6 + c], f, 2 * via + k)
+
+    def relay_in(k):
+        o = 2 * ((y + 2) % 4) + k
+        return pltpu.make_async_copy(X.at[rows_of(o)], X.at[rows_of(o)], ar.at[6 + k])
+
+    relay_out().start()
+    for n in (0, 2, 1, 3, 4):
+        near(n).start()
+
+    def r_x(e):
+        return remote(R.at[t], R.at[t], rs_.at[e - 1], rr.at[e - 1], f, (t + e) % 8)
+
+    for e in range(1, 8):
+        r_x(e).start()
 
     def p_a(e):
         return remote(PB.at[own], PB.at[own], ps.at[e - 1], pr.at[e - 1], fa(e), t)
@@ -122,13 +181,10 @@
             w_a0(W, s, r, d).wait_recv()
         for d in (0, 1):
             w_a2(W, s, r, d).start()
-        pump_b(W, s, r, 1)
-        pump_b(W, s, r, 2)
 
     def pump_a2(W, s, r):
         for d in (0, 1):
             w_a2(W, s, r, d).wait_recv()
-        pump_b(W, s, r, 3)
 
     def pump_b1(W, s, r, n):
         for d in (0, 1):
@@ -142,33 +198,22 @@
     U = (UB, us, ur)
     V = (DB, ds_, dr)
     pump_a0(*U)
-
-    ri = lax.broadcasted_iota(jnp.int32, (128, 128), 0)
-    ci = lax.broadcasted_iota(jnp.int32, (128, 128), 1)
-    eye = (ri == ci).astype(F32)
-
-    def to_lanes(col):
-        return jnp.sum(col * eye, axis=0, keepdims=True)
-
-    def to_column(lanes):
-        return jnp.sum(lanes * eye, axis=1, keepdims=True)
-
-    v = tokv[...].astype(F32)
-    r1 = lax.rsqrt(jnp.sum(v * v, axis=1, keepdims=True) / D + EPS)
-    R[t] = jnp.broadcast_to(to_lanes(r1), (8, 128))
-
-    def r_x(e):
-        return remote(R.at[t], R.at[t], rs_.at[e - 1], rr.at[e - 1], f, (t + e) % 8)
-
-    for e in range(1, 8):
-        r_x(e).start()
-
+    pump_b(*U, 0)
+    pump_a0(*V)
+
+    ph("d_wait_pa")
     for e in (1, 3, 2):
         p_a(e).wait_recv()
     for e in (1, 3, 2):
         p_b(e).start()
-    pump_b(*U, 0)
+    ph("d_relay")
+    relay_out().wait_recv()
+    for k in (0, 1):
+        relay_on(k).start()
+    ph("e_U_a1")
     pump_a1(*U)
+    pump_b(*U, 1)
+    pump_b(*U, 2)
 
     def row_of(ref):
         return jnp.concatenate([ref[pl.ds(2 * t, 1), :], ref[pl.ds(2 * t + 1, 1), :]], axis=1)
@@ -176,11 +221,15 @@
     gm = row_of(gmix)
     NB[pl.ds(0, 16), :] = jnp.zeros((16, 256), BF16)
     NB[pl.ds(16 + SEQ, 16), :] = jnp.zeros((16, 256), BF16)
+    ph("f_wait_x")
     c_x.wait()
-    c_d.wait()
-    for e in range(1, 8):
-        a2a(e).wait_recv()
+    for e in range(1, 8):
         r_x(e).wait_recv()
+    for n in range(5):
+        near_in(n).wait()
+    for k in (0, 1):
+        relay_in(k).wait()
+    ph("g_normed")
     for i in range(8):
         rc = to_column(R[i, 0:1, :])
         xv = X[pl.ds(128 * i, 128), :].astype(F32)
@@ -196,6 +245,7 @@
         ref = PL2.at[c, pl.ds(CH * q, CH)]
         return remote(ref, ref, xs.at[q], xr.at[q], f, sib)
 
+    ph("h_pool")
     for i in range(8):
         sums = jnp.dot(band, NB[pl.ds(128 * i, 160), :], preferred_element_type=F32)
         pos = 128 * i + lax.broadcasted_iota(jnp.int32, (128, 256), 0)
@@ -205,10 +255,10 @@
         if i % 2 == 1:
             pl_x(i // 2).start()
 
-    pump_a2(*U)
+    ph("i_pb")
     for e in (1, 3, 2):
         p_b(e).wait_recv()
-
+    ph("j_mix")
     psc = row_of(pscale)
     gml = row_of(gmlp)
 
@@ -243,6 +293,7 @@
         for h in (0, 1):
             SQ[t, pl.ds(2 * q + h, 1), :] = to_lanes(sq[128 * h:128 * h + 128])
 
+    ph("k_sq")
     def sq_x(e):
         return remote(SQ.at[t], SQ.at[t], ss.at[e - 1], sr.at[e - 1], f, (t + e) % 8)
 
@@ -263,127 +314,180 @@
         g_fwd(q).wait_recv()
         g_sib(3, q).start()
 
+    ph("l_Ua2")
+    pump_a2(*U)
+    pump_b(*U, 3)
     pump_b1(*U, 0)
+    ph("l_Va1")
+    pump_a1(*V)
+    ph("m_Ub1")
+    pump_b1(*U, 1)
+    ph("m_g0")
     g_pump(0)
-    pump_b1(*U, 1)
+    ph("m_Ub2")
+    pump_b1(*U, 2)
+    ph("m_g1")
     g_pump(1)
-    pump_b1(*U, 2)
+    ph("n_Ub3")
     pump_b1(*U, 3)
-    pump_a0(*V)
     pump_b(*V, 0)
+    pump_b(*V, 1)
+    ph("n_Va2")
+    pump_a2(*V)
+
+    @pl.when(c == 1)
+    def _():
+        pump_b(*V, 2)
+        pump_b(*V, 3)
+
+    ph("o_g2")
     g_pump(2)
+    ph("o_g3")
+    g_pump(3)
+    ph("o_g20")
     g_pump2(0)
-    g_pump(3)
-    g_pump2(1)
     g_pump2(2)
+    ph("p_Ub2")
     for n in range(4):
         pump_b2(*U, n)
-    pump_a1(*V)
-    g_pump2(3)
-
     for e in range(1, 8):
         sq_x(e).wait_recv()
     total = SQ[0]
     for i in range(1, 8):
         total = total + SQ[i]
     RT[...] = lax.rsqrt(total / D + EPS)
-    for k in range(4):
-        for q in range(NCH):
+
+    def up_rows(q):
+        for k in range(4):
             g_sib(k, q).wait_recv()
-
-    def up_rows(q, carry):
-        base = pl.multiple_of(CH * q, CH)
-        rows = pl.ds(base, CH)
-        rc = jnp.concatenate([to_column(RT[pl.ds(2 * q + h, 1), :]) for h in (0, 1)], axis=0)
+        ph(f"t_up{q}")
+        rows = pl.ds(CH * q, CH)
+        rc = jnp.concatenate([to_column(RT[2 * q + h:2 * q + h + 1, :]) for h in (0, 1)], axis=0)
         lhs = jnp.concatenate([G[i, rows, :] for i in range(8)], axis=1)
-
-        def cols(h, carry):
-            hs = pl.ds(pl.multiple_of(256 * h, 256), 256)
-            rhs = jnp.concatenate([UB[slot_of(g), hs, :] for g in range(16)], axis=1)
-            pre = lax.dot_general(lhs, rhs, (((1,), (1,)), ((), ())), preferred_element_type=F32)
-            act = jnp.maximum(pre * rc, 0.0)
-            H[rows, hs] = (act * act).astype(BF16)
-            return carry
-
-        return lax.fori_loop(0, 4, cols, carry)
-
-    lax.fori_loop(0, NCH, up_rows, 0)
-    pump_a2(*V)
-    for n in range(4):
-        pump_b1(*V, n)
-    for n in range(4):
-        pump_b2(*V, n)
-
-    def so(k, d):
-        return SO.at[k, d]
-
+        rhs = jnp.concatenate([UB[slot_of(g)] for g in range(16)], axis=1)
+        pre = lax.dot_general(lhs, rhs, (((1,), (1,)), ((), ())), preferred_element_type=F32)
+        act = jnp.maximum(pre * rc, 0.0)
+        H[rows, :] = (act * act).astype(BF16)
+
+    ph("s_gsib0")
+    up_rows(0)
+    ph("u_Vb0")
+    pump_b1(*V, 0)
+
+    @pl.when(c == 0)
+    def _():
+        pump_b(*V, 2)
+
+    ph("s_gsib2")
+    up_rows(2)
+    ph("s_g21")
+    g_pump2(1)
+    g_pump2(3)
+    ph("s_gsib1")
+    up_rows(1)
+    ph("u_Vb1")
+    pump_b1(*V, 1)
+
+    @pl.when(c == 0)
+    def _():
+        pump_b(*V, 3)
+
+    ph("s_gsib3")
+    up_rows(3)
+
+    ph("w_down")
     def c_x2(k, d):
         return remote(SO.at[k, d], SB.at[k, d], cs.at[4 * k + d], cr.at[4 * k + d], f, sib)
 
     def y_half(k, d):
         return remote(SO.at[k, 2, hrows[d]], RH.at[k, d], ys.at[4 * k + d], yr.at[4 * k + d], f, yp if d == 0 else ym)
 
-    def y_full(k, d):
-        return remote(SO.at[k, 1 if d == 0 else 3], RY.at[k, d], ys.at[4 * k + 2 + d], yr.at[4 * k + 2 + d], f,
-                      yp if d == 0 else ym)
-
-    for k in range(4):
+    def y_now(k, d):
+        return remote(SO.at[k, 1 + 2 * d, hrows[1 - d]], RY.at[k, d, hrows[1 - d]], ys.at[4 * k + 2 + d],
+                      yr.at[4 * k + 2 + d], f, yp if d == 0 else ym)
+
+    def y_late(k, d):
+        return remote(SO.at[k, 1 + 2 * d, hrows[d]], RY.at[k, d, hrows[d]], ys.at[16 + 2 * k + d],
+                      yr.at[16 + 2 * k + d], f, yp if d == 0 else ym)
+
+    def ready(k):
+        @pl.when(c == 0)
+        def _():
+            if k >= 2:
+                pump_b1(*V, k)
+            pump_b2(*V, k)
+
+        @pl.when(c == 1)
+        def _():
+            if k == 1:
+                pump_b1(*V, 2)
+                pump_b1(*V, 3)
+            if k == 3:
+                for n in range(4):
+                    pump_b2(*V, n)
+
+    def roles(k):
         xk = (x + offs[k]) % 4
-        owner = xk // 2 == c
-        helper = xk // 2 != c
-        half = xk % 2
-
-        def down(q, carry):
-            rows = pl.ds(pl.multiple_of(CH * q, CH), CH)
-            rhs = jnp.concatenate([DB[slot_of(4 * ((y + d) % 4) + xk)] for d in range(4)], axis=1)
-            PART[rows, :] = jnp.dot(H[rows, :], rhs, preferred_element_type=F32)
-            return carry
-
-        lax.fori_loop(0, NCH, down, 0)
+        return xk, xk // 2 == c, xk // 2 != c
+
+    def down(k):
+        xk, _, _ = roles(k)
+        rhs = jnp.concatenate([DB[slot_of(4 * ((y + d) % 4) + xk)] for d in range(4)], axis=1)
+        PART[k % 2] = jnp.dot(H[...], rhs, preferred_element_type=F32)
+
+    def both(k, d, rows):
+        return PART[k % 2, rows, 128 * d:128 * d + 128] + SB[k, d, rows].astype(F32)
+
+    def stage1(k):
+        _, owner, helper = roles(k)
 
         @pl.when(helper)
         def _():
             for d in (2, 1, 3, 0):
-                SO[k, d] = PART[:, 128 * d:128 * d + 128].astype(BF16)
+                SO[k, d] = PART[k % 2, :, 128 * d:128 * d + 128].astype(BF16)
                 c_x2(k, d).start()
-            for d in (2, 1, 3, 0):
-                c_x2(k, d).wait_send()
 
         @pl.when(owner)
         def _():
             c_x2(k, 2).wait_recv()
-            SO[k, 2] = (PART[:, 256:384] + SB[k, 2].astype(F32)).astype(BF16)
-            y_half(k, 0).start()
-            y_half(k, 1).start()
-            c_x2(k, 1).wait_recv()
-            c_x2(k, 3).wait_recv()
-            y_half(k, 0).wait_recv()
-            SO[k, 1, hrows[0]] = (PART[hrows[0], 128:256] + SB[k, 1, hrows[0]].astype(F32)
-                                  + RH[k, 0].astype(F32)).astype(BF16)
-            SO[k, 1, hrows[1]] = (PART[hrows[1], 128:256] + SB[k, 1, hrows[1]].astype(F32)).astype(BF16)
-            y_full(k, 0).start()
-            y_half(k, 1).wait_recv()
-            SO[k, 3, hrows[0]] = (PART[hrows[0], 384:512] + SB[k, 3, hrows[0]].astype(F32)).astype(BF16)
-            SO[k, 3, hrows[1]] = (PART[hrows[1], 384:512] + SB[k, 3, hrows[1]].astype(F32)
-                                  + RH[k, 1].astype(F32)).astype(BF16)
-            y_full(k, 1).start()
+            for d in (0, 1):
+                SO[k, 2, hrows[d]] = both(k, 2, hrows[d]).astype(BF16)
+                y_half(k, d).start()
+            for d in (0, 1):
+                c_x2(k, 1 + 2 * d).wait_recv()
+                SO[k, 1 + 2 * d, hrows[1 - d]] = both(k, 1 + 2 * d, hrows[1 - d]).astype(BF16)
+                y_now(k, d).start()
+
+    def stage2(k):
+        xk, owner, _ = roles(k)
+
+        @pl.when(owner)
+        def _():
+            for d in (0, 1):
+                y_half(k, d).wait_recv()
+                SO[k, 1 + 2 * d, hrows[d]] = (both(k, 1 + 2 * d, hrows[d]) + RH[k, d].astype(F32)).astype(BF16)
+                y_late(k, d).start()
             c_x2(k, 0).wait_recv()
-            ACC[half] = ACC[half] + PART[:, 0:128] + SB[k, 0].astype(F32)
-
-    for k in range(4):
-        xk = (x + offs[k]) % 4
-        owner = xk // 2 == c
-        half = xk % 2
+            for h in (0, 1):
+                ACC[xk % 2, hrows[h]] = ACC[xk % 2, hrows[h]] + both(k, 0, hrows[h])
+
+    def stage3(k):
+        xk, owner, _ = roles(k)
 
         @pl.when(owner)
         def _():
-            y_full(k, 0).wait_recv()
-            y_full(k, 1).wait_recv()
-            ACC[half] = ACC[half] + RY[k, 0].astype(F32) + RY[k, 1].astype(F32)
             for d in (0, 1):
-                y_half(k, d).wait_send()
-                y_full(k, d).wait_send()
-
+                y_now(k, d).wait_recv()
+                y_late(k, d).wait_recv()
+            ACC[xk % 2] = ACC[xk % 2] + RY[k, 0].astype(F32) + RY[k, 1].astype(F32)
+
+    for step in ("r0", "d0", "10", "20", "r1", "d1", "11", "r2", "d2", "21", "12", "r3", "22", "d3", "13",
+                 "30", "31", "32", "23", "33"):
+        k = int(step[1])
+        ph("w_" + step)
+        {"r": ready, "d": down, "1": stage1, "2": stage2, "3": stage3}[step[0]](k)
+
+    ph("y_sq2")
     for i in range(8):
         rows = pl.ds(128 * i, 128)
         a0, a1 = ACC[0, rows, :], ACC[1, rows, :]
@@ -394,6 +498,7 @@
 
     for e in range(1, 8):
         t_x(e).start()
+    ph("y_wait")
     for e in range(1, 8):
         t_x(e).wait_recv()
     total = SQ2[0]
@@ -406,11 +511,31 @@
         for h in (0, 1):
             out[rows, 128 * h:128 * h + 128] = (ACC[h, rows, :] * rc * gout[h:h + 1, :]).astype(BF16)
 
-    for e in range(1, 8):
-        a2a(e).wait_send()
+    ph("z_sent")
+    relay_out().wait_send()
+    for k in (0, 1):
+        relay_on(k).wait_send()
+    for n in range(5):
+        near(n).wait_send()
+    for e in range(1, 8):
         r_x(e).wait_send()
         sq_x(e).wait_send()
         t_x(e).wait_send()
+    for k in range(4):
+        _, owner, helper = roles(k)
+
+        @pl.when(owner)
+        def _():
+            for d in (0, 1):
+                y_half(k, d).wait_send()
+                y_now(k, d).wait_send()
+                y_late(k, d).wait_send()
+
+        @pl.when(helper)
+        def _():
+            for d in range(4):
+                c_x2(k, d).wait_send()
+
     for e in (1, 2, 3):
         p_a(e).wait_send()
         p_b(e).wait_send()
@@ -428,6 +553,7 @@
         g_fwd(q).wait_send()
         for k in range(4):
             g_sib(k, q).wait_send()
+    ph(None)
 
 
 def local(tokens, pool_weight, pool_scale, gain_mix, gain_mlp, w_up, w_down, gain_out):
@@ -441,6 +567,7 @@
         out_specs=vmem,
         scratch_shapes=[
             pltpu.VMEM((128, D), BF16),
+            pltpu.VMEM((128, 512), BF16),
             pltpu.VMEM((SEQ, 256), BF16),
             pltpu.VMEM((SEQ + 32, 256), BF16),
             pltpu.VMEM((8, 8, 128), F32),
@@ -453,14 +580,14 @@
             pltpu.VMEM((8, 8, 128), F32),
             pltpu.VMEM((8, 8, 128), F32),
             pltpu.VMEM((SEQ, 1024), BF16),
-            pltpu.VMEM((SEQ, 512), F32),
+            pltpu.VMEM((2, SEQ, 512), F32),
             pltpu.VMEM((4, 4, SEQ, 128), BF16),
             pltpu.VMEM((4, 4, SEQ, 128), BF16),
             pltpu.VMEM((4, 2, HALF, 128), BF16),
             pltpu.VMEM((4, 2, SEQ, 128), BF16),
             pltpu.VMEM((2, SEQ, 128), F32),
             dma((5,)),
-            dma((7,)), dma((7,)),
+            dma((8,)), dma((8,)),
             dma((7,)), dma((7,)),
             dma((6,)), dma((6,)),
             dma((20,)), dma((20,)),
@@ -470,7 +597,7 @@
             dma((7,)), dma((7,)),
             dma((7,)), dma((7,)),
             dma((16,)), dma((16,)),
-            dma((16,)), dma((16,)),
+            dma((24,)), dma((24,)),
         ],
         compiler_params=pltpu.CompilerParams(
             collective_id=0, has_side_effects=True, vmem_limit_bytes=60 * 1024 * 1024),

time: 107 us -> 86.5 us (0.81); the launches traced: 107 us -> 85.3 us
  Pallas kernels: 105 us -> 83.4 us
    pallas_call x1, Pallas kernels: 105 us -> 83.4 us  [local(): pl.pallas_call(kernel, out_shape=jax.ShapeDtypeStruct((SEQ, 256), BF16),...]
where the time goes in v2:
time: 86.5 us; the launch traced here: 85.3 us
  Pallas kernels  83.4 us (96%)
  local copies, waits for them, and re-layouts  1.87 us (2%)
    pallas_call x1, Pallas kernels, local(): pl.pallas_call(kernel, out_shape=jax.ShapeDtypeStruct((SEQ, 256), BF16),...  83.4 us
    unnamed x1, local copies, waits for them, and re-layouts  1.87 us

profile of v2, /device:TPU:1, one launch (start us, length us, event | category | flops | bytes accessed | tf_op | source)
XLA Modules:
  0.0 85.3 jit_solution(16170082287651149412)
XLA Ops:
  0.0 83.4 %mixers.1 = bf16[1024,256]{1,0:T(8,128)(2,1)} custom-call(bf16[128,2048]{1,0:T(8,128)(2,1)} %tok.1, bf16[4,32,512]{2,1,0:T(8,128)(2,1)} %pw.1, bf16[1024,128]{1,0:T(8,128)(2,1)} %up.1, bf16[1024,128]{1,0:T(8,128)(2,1)} %dn.1, f32[16,128]{1,0:T(8,128)} %bitcast.4, f32[16,128]{1,0:T(8,128)} %bitcast.5, f32[16,128]{1,0:T(8,128)} %bitcast.6, f32[2,128]{1,0:T(2,128)} %bitcast.7), custom_call_target="tpu_custom_call" | custom-call | tf_op jit(solution)/shard_map/mixers/pallas_call | solution.py:563
  83.4 1.9 %copy.10 = bf16[1024,256]{1,0:T(8,128)(2,1)} copy(bf16[1024,256]{1,0:T(8,128)(2,1)} %mixers.1) | data formatting | bytes 1048576

commit v3 on v2

v3 whole, which is shorter than its diff:
```python
import functools

import jax
import jax.numpy as jnp
from jax import lax
from jax.experimental import pallas as pl
from jax.experimental.pallas import tpu as pltpu
from jax.sharding import PartitionSpec as P

D = 2048
SEQ = 1024
EPS = 1e-06
F32 = jnp.float32
BF16 = jnp.bfloat16
MESH = pl.DeviceIdType.MESH
CH = 256
NCH = SEQ // CH
HALF = SEQ // 2


class Phases:
    now = None

    def __call__(self, name):
        if self.now is not None:
            self.now.__exit__(None, None, None)
        self.now = jax.named_scope(name) if name else None
        if name:
            self.now.__enter__()


def kernel(tok, pw, up, dn, pscale_h, gmix_h, gmlp_h, gout_h, out,
           tokv, RL, X, NB, R, RT, PB, UB, DB, PL2, G, SQ, SQ2, H, PART, SS, SB, SO, RH, RY, RZ, ACC,
           pscale, gmix, gmlp, gout, lsem, snd, rcv):
    ph = Phases()
    f = lax.axis_index("fs")
    t = lax.axis_index("tp")
    z, x = f // 4, f % 4
    y, c = t // 2, t % 2

    def fa(d):
        return (1 - c) * (4 * z + (x + d) % 4) + c * (4 * ((z + d) % 4) + x)

    def fb(d):
        return (1 - c) * (4 * ((z + d) % 4) + x) + c * (4 * z + (x + d) % 4)

    pa = (1 - c) * x + c * z
    pb = (1 - c) * z + c * x

    def slot(i, j):
        return 4 * ((pb + j) % 4) + (pa + i) % 4

    def slot_of(g):
        return (1 - c) * g + c * (4 * (g % 4) + g // 4)

    def remote(src, dst, ssem, rsem, fs, tp):
        return pltpu.make_async_remote_copy(
            src_ref=src, dst_ref=dst, send_sem=snd.at[ssem], recv_sem=rcv.at[rsem],
            device_id={"fs": fs, "tp": tp}, device_id_type=MESH)

    def arrived(ref, rsem):
        pltpu.make_async_copy(ref, ref, rcv.at[rsem]).wait()

    sib = 2 * y + 1 - c
    yp = 2 * ((y + 1) % 4) + c
    ym = 2 * ((y + 3) % 4) + c
    own = slot(0, 0)

    ph("a_entry")
    c_tok = pltpu.make_async_copy(tok, tokv, lsem.at[0])
    c_x = pltpu.make_async_copy(
        tok.at[:, pl.ds(pl.multiple_of(256 * t, 256), 256)],
        X.at[pl.ds(pl.multiple_of(128 * t, 128), 128)], lsem.at[1])
    c_u = pltpu.make_async_copy(up, UB.at[own], lsem.at[2])
    c_d = pltpu.make_async_copy(dn, DB.at[own], lsem.at[3])
    c_p = pltpu.make_async_copy(
        pw.at[y, :, pl.ds(pl.multiple_of(256 * c, 256), 256)], PB.at[own], lsem.at[4])
    c_g = [pltpu.make_async_copy(h, v, lsem.at[5 + i])
           for i, (h, v) in enumerate(((pscale_h, pscale), (gmix_h, gmix), (gmlp_h, gmlp), (gout_h, gout)))]
    for cp in [c_tok, c_p, c_u, c_x, c_d] + c_g:
        cp.start()
    barrier = pltpu.get_barrier_semaphore()
    for e in range(1, 8):
        pl.semaphore_signal(barrier, inc=1, device_id={"fs": f, "tp": (t + e) % 8}, device_id_type=MESH)
    for e in (1, 2, 3):
        pl.semaphore_signal(barrier, inc=1, device_id={"fs": fa(e), "tp": t}, device_id_type=MESH)
        pl.semaphore_signal(barrier, inc=1, device_id={"fs": fb(e), "tp": t}, device_id_type=MESH)

    ri = lax.broadcasted_iota(jnp.int32, (128, 128), 0)
    ci = lax.broadcasted_iota(jnp.int32, (128, 128), 1)
    eye = (ri == ci).astype(F32)

    def to_lanes(col):
        return jnp.sum(col * eye, axis=0, keepdims=True)

    def to_column(lanes):
        return jnp.sum(lanes * eye, axis=1, keepdims=True)

    c_tok.wait()
    v = tokv[...].astype(F32)
    r1 = lax.rsqrt(jnp.sum(v * v, axis=1, keepdims=True) / D + EPS)
    R[t] = jnp.broadcast_to(to_lanes(r1), (8, 128))
    c_p.wait()
    c_u.wait()
    c_d.wait()
    pl.semaphore_wait(barrier, 13)

    ph("b_start")
    via = (y + 1 + 2 * c) % 4

    def rows_of(o):
        return pl.ds(pl.multiple_of(128 * o, 128), 128)

    def near(n):
        p = (2 * ((y + (1 if n < 2 else 3)) % 4) + n % 2) if n < 4 else sib
        return remote(tokv.at[:, pl.ds(pl.multiple_of(256 * p, 256), 256)], X.at[rows_of(t)], 0, 0, f, p)

    def relay_out():
        return remote(tokv.at[:, pl.ds(pl.multiple_of(512 * ((y + 2) % 4), 512), 512)], RL, 0, 1, f, 2 * via + c)

    def relay_on(k):
        o = 2 * ((y + 3 + 2 * c) % 4) + c
        return remote(RL.at[:, pl.ds(256 * k, 256)], X.at[rows_of(o)], 0, 0, f, 2 * via + k)

    relay_out().start()
    for n in (0, 2, 1, 3, 4):
        near(n).start()

    def r_x(e):
        return remote(R.at[t], R.at[t], 1, 2, f, (t + e) % 8)

    for e in range(1, 8):
        r_x(e).start()

    def p_a(e):
        return remote(PB.at[own], PB.at[own], 1, 3, fa(e), t)

    def p_b(e):
        line = PB.at[pl.ds(4 * pb, 4)]
        return remote(line, line, 1, 4, fb(e), t)

    for e in (1, 3, 2):
        p_a(e).start()

    hrows = (pl.ds(0, HALF), pl.ds(HALF, HALF))
    offs = (0, 3, 1, 2)

    def w_a0(W, s, r, d):
        ref = W.at[own]
        return remote(ref, ref, s, r, fa(1 if d == 0 else 3), t)

    def w_a2(W, s, r, d):
        ref = W.at[slot(3 if d == 0 else 1, 0), hrows[d]]
        return remote(ref, ref, s, r + 1, fa(1 if d == 0 else 3), t)

    def w_b(W, s, r, n, d):
        ref = W.at[slot(offs[n], 0)]
        return remote(ref, ref, s, r + 2 + n, fb(1 if d == 0 else 3), t)

    def w_b2(W, s, r, n, d):
        ref = W.at[slot(offs[n], 3 if d == 0 else 1), hrows[d]]
        return remote(ref, ref, s, r + 6 + n, fb(1 if d == 0 else 3), t)

    def pump_a0(W, s, r):
        for d in (0, 1):
            w_a0(W, s, r, d).start()

    def pump_b(W, s, r, n):
        for d in (0, 1):
            w_b(W, s, r, n, d).start()

    def pump_a1(W, s, r):
        arrived(W.at[pl.ds(0, 2)], r)
        for d in (0, 1):
            w_a2(W, s, r, d).start()

    def pump_a2(W, s, r):
        arrived(W.at[0], r + 1)

    def pump_b1(W, s, r, n):
        arrived(W.at[pl.ds(0, 2)], r + 2 + n)
        for d in (0, 1):
            w_b2(W, s, r, n, d).start()

    def pump_b2(W, s, r, n):
        arrived(W.at[0], r + 6 + n)

    U = (UB, 2, 5)
    V = (DB, 3, 15)
    pump_a0(*U)
    pump_b(*U, 0)

    ph("d_wait_pa")
    arrived(PB.at[pl.ds(0, 3)], 3)
    for e in (1, 3, 2):
        p_b(e).start()
    ph("d_relay")
    arrived(RL, 1)
    for k in (0, 1):
        relay_on(k).start()
    ph("e_Ua1")
    pump_a1(*U)
    pump_b(*U, 1)
    pump_b(*U, 2)
    def row_of(ref):
        return jnp.concatenate([ref[pl.ds(2 * t, 1), :], ref[pl.ds(2 * t + 1, 1), :]], axis=1)

    NB[pl.ds(0, 16), :] = jnp.zeros((16, 256), BF16)
    NB[pl.ds(16 + SEQ, 16), :] = jnp.zeros((16, 256), BF16)
    ph("f_wait_x")
    c_x.wait()
    for cp in c_g:
        cp.wait()
    gm = row_of(gmix)
    arrived(R.at[pl.ds(0, 7)], 2)
    arrived(X.at[pl.ds(0, 896)], 0)
    ph("g_normed")
    for i in range(8):
        rc = to_column(R[i, 0:1, :])
        xv = X[pl.ds(128 * i, 128), :].astype(F32)
        NB[pl.ds(16 + 128 * i, 128), :] = (xv * rc * gm).astype(BF16)

    reach = 1 + (y >= 1).astype(jnp.int32) + 2 * (y >= 2).astype(jnp.int32) + 4 * (y >= 3).astype(jnp.int32)
    bi = lax.broadcasted_iota(jnp.int32, (128, 160), 0)
    bj = lax.broadcasted_iota(jnp.int32, (128, 160), 1)
    delta = bj - 16 - bi
    band = jnp.where((delta >= -reach) & (delta < reach), 1.0, 0.0).astype(BF16)

    def pl_x(q):
        ref = PL2.at[c, pl.ds(CH * q, CH)]
        return remote(ref, ref, 4, 25 + q, f, sib)

    ph("h_pool")
    for i in range(8):
        sums = jnp.dot(band, NB[pl.ds(128 * i, 160), :], preferred_element_type=F32)
        pos = 128 * i + lax.broadcasted_iota(jnp.int32, (128, 256), 0)
        count = jnp.minimum(pos + reach, SEQ) - jnp.maximum(pos - reach, 0)
        mine = NB[pl.ds(16 + 128 * i, 128), :].astype(F32)
        PL2[c, pl.ds(128 * i, 128), :] = (sums / count.astype(F32) - mine).astype(BF16)
        if i % 2 == 1:
            pl_x(i // 2).start()

    ph("i_pb")
    arrived(PB.at[pl.ds(0, 12)], 4)
    ph("j_mix")
    psc = row_of(pscale)
    gml = row_of(gmlp)

    def g_ref(owner, q):
        return G.at[owner, pl.ds(CH * q, CH)]

    def g_y(q, d):
        return remote(g_ref(t, q), g_ref(t, q), 5, 29 + q, f, yp if d == 0 else ym)

    def g_sib(k, q):
        owner = (t + (0, 6, 2, 4)[k]) % 8
        return remote(g_ref(owner, q), g_ref(owner, q), 5, 35 + q, f, sib)

    def g_fwd(q):
        owner = ym if q < 2 else yp
        return remote(g_ref(owner, q), g_ref(owner, q), 5, 33 + q % 2, f, yp if q < 2 else ym)

    pk = [jnp.concatenate([PB[slot_of(8 * k + i)] for i in range(8)], axis=0) for k in (0, 1)]
    for q in range(NCH):
        arrived(PL2.at[1 - c, pl.ds(CH * q, CH)], 25 + q)
        rows = pl.ds(CH * q, CH)
        mixed = (jnp.dot(PL2[0, rows, :], pk[0], preferred_element_type=F32)
                 + jnp.dot(PL2[1, rows, :], pk[1], preferred_element_type=F32)) * psc
        first = (X[rows, :].astype(F32) + mixed).astype(BF16).astype(F32)
        G[t, rows, :] = (first * gml).astype(BF16)
        for d in (0, 1):
            g_y(q, d).start()
        g_sib(0, q).start()
        ACC[0, rows, :] = first[:, :128]
        ACC[1, rows, :] = first[:, 128:]
        sq = jnp.sum(first * first, axis=1, keepdims=True)
        for h in (0, 1):
            SQ[t, pl.ds(2 * q + h, 1), :] = to_lanes(sq[128 * h:128 * h + 128])

    ph("k_sq")
    def sq_x(e):
        return remote(SQ.at[t], SQ.at[t], 1, 39, f, (t + e) % 8)

    for e in range(1, 8):
        sq_x(e).start()

    def g_pump(q):
        arrived(G.at[0, pl.ds(0, 2 * CH)], 29 + q)
        g_fwd(q).start()
        g_sib(1, q).start()
        g_sib(2, q).start()

    def g_pump2(q):
        arrived(G.at[0, pl.ds(0, 2 * CH)], 33 + q)
        g_sib(3, q).start()
        g_sib(3, q + 2).start()

    ph("l_Ub0")
    pump_b1(*U, 0)
    ph("l_Ua2")
    pump_a2(*U)
    pump_b(*U, 3)
    ph("m_Ub1")
    pump_b1(*U, 1)
    pump_a0(*V)
    ph("m_g0")
    g_pump(0)
    ph("m_g1")
    g_pump(1)
    ph("m_Ub2")
    pump_b1(*U, 2)
    ph("m_g2")
    g_pump(2)
    ph("n_Ub3")
    pump_b1(*U, 3)
    pump_b(*V, 0)
    ph("n_Va1")
    pump_a1(*V)
    pump_b(*V, 1)

    @pl.when(c == 1)
    def _():
        pump_b(*V, 2)

    ph("o_g3")
    g_pump(3)
    ph("o_g20")
    g_pump2(0)
    ph("p_Ub2")
    for n in range(4):
        pump_b2(*U, n)
    ph("p_g21")
    g_pump2(1)
    ph("p_Va2")
    pump_a2(*V)

    @pl.when(c == 1)
    def _():
        pump_b(*V, 3)

    arrived(SQ.at[pl.ds(0, 7)], 39)
    total = SQ[0]
    for i in range(1, 8):
        total = total + SQ[i]
    RT[...] = lax.rsqrt(total / D + EPS)

    def up_rows(q):
        arrived(G.at[pl.ds(0, 4), pl.ds(0, CH)], 35 + q)
        ph(f"t_up{q}")
        rows = pl.ds(CH * q, CH)
        rc = jnp.concatenate([to_column(RT[2 * q + h:2 * q + h + 1, :]) for h in (0, 1)], axis=0)
        lhs = jnp.concatenate([G[i, rows, :] for i in range(8)], axis=1)
        rhs = jnp.concatenate([UB[slot_of(g)] for g in range(16)], axis=1)
        pre = lax.dot_general(lhs, rhs, (((1,), (1,)), ((), ())), preferred_element_type=F32)
        act = jnp.maximum(pre * rc, 0.0)
        H[rows, :] = (act * act).astype(BF16)

    ph("s_gsib0")
    up_rows(0)
    ph("s_gsib2")
    up_rows(2)
    ph("u_Vb0")
    pump_b1(*V, 0)

    @pl.when(c == 0)
    def _():
        pump_b(*V, 2)

    ph("s_gsib1")
    up_rows(1)
    ph("u_Vb1")
    pump_b1(*V, 1)

    @pl.when(c == 0)
    def _():
        pump_b(*V, 3)

    ph("s_gsib3")
    up_rows(3)

    mine, other = pl.ds(pl.multiple_of(HALF * c, HALF), HALF), pl.ds(pl.multiple_of(HALF * (1 - c), HALF), HALF)
    quarter = HALF // 2
    qrows = (pl.ds(0, quarter), pl.ds(quarter, quarter))

    def column(k):
        xk = (x + offs[k]) % 4
        return xk, xk // 2

    def c_x2(k, d):
        return remote(SS.at[k, d], SB.at[k, d], 4, 40 + 4 * k + d, f, sib)

    def y_half(k, d):
        return remote(SO.at[k, 2, qrows[d]], RH.at[k, d], 6, 56 + 2 * k + d, f, yp if d == 0 else ym)

    def y_part(k, d, h):
        to = 2 * ((y + 1 + 2 * d) % 4) + column(k)[1]
        rows = pl.ds(pl.multiple_of(HALF * c + quarter * h, quarter), quarter)
        return remote(SO.at[k, 1 + 2 * d, qrows[h]], RY.at[k, d, rows], 6, 64 + k, f, to)

    def z_x(k):
        return remote(SO.at[k, 0], RZ.at[k], 4, 68 + k, f, sib)

    def ready(k):
        @pl.when(c == 0)
        def _():
            if k in (1, 2):
                pump_b1(*V, k + 1)
            pump_b2(*V, k)

        @pl.when(c == 1)
        def _():
            if k == 1:
                pump_b1(*V, 2)
                pump_b1(*V, 3)
            if k == 3:
                for n in range(4):
                    pump_b2(*V, n)

    def down(k):
        xk, _ = column(k)
        rhs = jnp.concatenate([DB[slot_of(4 * ((y + d) % 4) + xk)] for d in range(4)], axis=1)
        part = jnp.dot(H[other, :], rhs, preferred_element_type=F32)
        for d in (2, 1, 3, 0):
            SS[k, d] = part[:, 128 * d:128 * d + 128].astype(BF16)
            c_x2(k, d).start()
        PART[k % 2] = jnp.dot(H[mine, :], rhs, preferred_element_type=F32)

    def both(k, d, rows):
        return PART[k % 2, rows, 128 * d:128 * d + 128] + SB[k, d, rows].astype(F32)

    def stage1(k):
        arrived(SB.at[k, 2], 40 + 4 * k + 2)
        for d in (0, 1):
            SO[k, 2, qrows[d]] = both(k, 2, qrows[d]).astype(BF16)
            y_half(k, d).start()
        for d in (0, 1):
            b = 1 + 2 * d
            arrived(SB.at[k, b], 40 + 4 * k + b)
            SO[k, b, qrows[1 - d]] = both(k, b, qrows[1 - d]).astype(BF16)
            y_part(k, d, 1 - d).start()

    def stage2(k):
        xk, keeper = column(k)
        for d in (0, 1):
            b = 1 + 2 * d
            arrived(RH.at[k, d], 56 + 2 * k + d)
            SO[k, b, qrows[d]] = (both(k, b, qrows[d]) + RH[k, d].astype(F32)).astype(BF16)
            y_part(k, d, d).start()
        arrived(SB.at[k, 0], 40 + 4 * k)

        @pl.when(keeper == c)
        def _():
            ACC[xk % 2, mine] = ACC[xk % 2, mine] + both(k, 0, pl.ds(0, HALF))

        @pl.when(keeper != c)
        def _():
            SO[k, 0] = both(k, 0, pl.ds(0, HALF)).astype(BF16)
            z_x(k).start()

    def stage3(k):
        xk, keeper = column(k)

        @pl.when(keeper == c)
        def _():
            arrived(RZ.at[k], 68 + k)
            ACC[xk % 2, other] = ACC[xk % 2, other] + RZ[k].astype(F32)
            arrived(RY.at[k], 64 + k)
            ACC[xk % 2] = ACC[xk % 2] + RY[k, 0].astype(F32) + RY[k, 1].astype(F32)

    for step in ("r0", "d0", "10", "r1", "d1", "11", "20", "r2", "d2", "12", "21", "r3", "d3", "13",
                 "22", "30", "23", "31", "32", "33"):
        k = int(step[1])
        ph("w_" + step)
        {"r": ready, "d": down, "1": stage1, "2": stage2, "3": stage3}[step[0]](k)

    ph("y_sq2")
    for i in range(8):
        rows = pl.ds(128 * i, 128)
        a0, a1 = ACC[0, rows, :], ACC[1, rows, :]
        SQ2[t, pl.ds(i, 1), :] = to_lanes(jnp.sum(a0 * a0 + a1 * a1, axis=1, keepdims=True))

    def t_x(e):
        return remote(SQ2.at[t], SQ2.at[t], 1, 72, f, (t + e) % 8)

    for e in range(1, 8):
        t_x(e).start()
    ph("y_wait")
    arrived(SQ2.at[pl.ds(0, 7)], 72)
    total = SQ2[0]
    for i in range(1, 8):
        total = total + SQ2[i]
    rl = lax.rsqrt(total / D + EPS)

    def out_x(q):
        rows = pl.ds(CH * q, CH)
        return pltpu.make_async_copy(X.at[rows], out.at[rows], lsem.at[q])

    for i in range(8):
        rows = pl.ds(128 * i, 128)
        rc = to_column(rl[i:i + 1, :])
        for h in (0, 1):
            X[rows, 128 * h:128 * h + 128] = (ACC[h, rows, :] * rc * gout[h:h + 1, :]).astype(BF16)
        if i % 2 == 1:
            out_x(i // 2).start()

    ph("z_sent")
    relay_out().wait_send()
    for k in (0, 1):
        relay_on(k).wait_send()
    for n in range(5):
        near(n).wait_send()
    for e in range(1, 8):
        r_x(e).wait_send()
        sq_x(e).wait_send()
        t_x(e).wait_send()
    for e in (1, 2, 3):
        p_a(e).wait_send()
        p_b(e).wait_send()
    for W in (U, V):
        for d in (0, 1):
            w_a0(*W, d).wait_send()
            w_a2(*W, d).wait_send()
            for n in range(4):
                w_b(*W, n, d).wait_send()
                w_b2(*W, n, d).wait_send()
    for q in range(NCH):
        pl_x(q).wait_send()
        g_y(q, 0).wait_send()
        g_y(q, 1).wait_send()
        g_fwd(q).wait_send()
        for k in range(4):
            g_sib(k, q).wait_send()
    for k in range(4):
        for d in range(4):
            c_x2(k, d).wait_send()
        for d in (0, 1):
            y_half(k, d).wait_send()
            y_part(k, d, 0).wait_send()
            y_part(k, d, 1).wait_send()

        @pl.when(column(k)[1] != c)
        def _():
            z_x(k).wait_send()

    for q in range(NCH):
        out_x(q).wait()
    ph(None)


def local(tokens, pool_weight, pool_scale, gain_mix, gain_mlp, w_up, w_down, gain_out):
    dma = pltpu.SemaphoreType.DMA
    hbm = pl.BlockSpec(memory_space=pltpu.HBM)
    return pl.pallas_call(
        kernel,
        out_shape=jax.ShapeDtypeStruct((SEQ, 256), BF16),
        in_specs=[hbm] * 8,
        out_specs=hbm,
        scratch_shapes=[
            pltpu.VMEM((128, D), BF16),
            pltpu.VMEM((128, 512), BF16),
            pltpu.VMEM((SEQ, 256), BF16),
            pltpu.VMEM((SEQ + 32, 256), BF16),
            pltpu.VMEM((8, 8, 128), F32),
            pltpu.VMEM((8, 128), F32),
            pltpu.VMEM((16, 32, 256), BF16),
            pltpu.VMEM((16, 1024, 128), BF16),
            pltpu.VMEM((16, 1024, 128), BF16),
            pltpu.VMEM((2, SEQ, 256), BF16),
            pltpu.VMEM((8, SEQ, 256), BF16),
            pltpu.VMEM((8, 8, 128), F32),
            pltpu.VMEM((8, 8, 128), F32),
            pltpu.VMEM((SEQ, 1024), BF16),
            pltpu.VMEM((2, HALF, 512), F32),
            pltpu.VMEM((4, 4, HALF, 128), BF16),
            pltpu.VMEM((4, 4, HALF, 128), BF16),
            pltpu.VMEM((4, 4, HALF, 128), BF16),
            pltpu.VMEM((4, 2, HALF // 2, 128), BF16),
            pltpu.VMEM((4, 2, SEQ, 128), BF16),
            pltpu.VMEM((4, HALF, 128), BF16),
            pltpu.VMEM((2, SEQ, 128), F32),
            pltpu.VMEM((16, 128), F32),
            pltpu.VMEM((16, 128), F32),
            pltpu.VMEM((16, 128), F32),
            pltpu.VMEM((2, 128), F32),
            dma((9,)),
            dma((7,)),
            dma((73,)),
        ],
        compiler_params=pltpu.CompilerParams(
            collective_id=0, has_side_effects=True, vmem_limit_bytes=60 * 1024 * 1024),
        name="mixers",
    )(tokens, pool_weight, w_up, w_down, pool_scale.reshape(16, 128), gain_mix.reshape(16, 128),
      gain_mlp.reshape(16, 128), gain_out.reshape(2, 128))


def solution(mesh):
    placed = (P(("fs", "tp"), None), P(None, "fs", None), P(), P(), P(), P("tp", "fs"), P("tp", "fs"), P("tp"))
    return jax.shard_map(local, mesh=mesh, in_specs=placed, out_specs=P("fs", "tp"), check_vma=False)
```

time: 86.5 us -> 75.7 us (0.88); the launches traced: 85.3 us -> 75.5 us
  Pallas kernels: 83.4 us -> 73.6 us
    pallas_call x1, Pallas kernels: 83.4 us -> 73.6 us  [local(): pl.pallas_call(kernel, out_shape=jax.ShapeDtypeStruct((SEQ, 256), BF16),...]
where the time goes in v3:
time: 75.7 us; the launch traced here: 75.5 us
  Pallas kernels  73.6 us (97%)
  local copies, waits for them, and re-layouts  1.87 us (2%)
    pallas_call x1, Pallas kernels, local(): pl.pallas_call(kernel, out_shape=jax.ShapeDtypeStruct((SEQ, 256), BF16),...  73.6 us
    unnamed x1, local copies, waits for them, and re-layouts  1.87 us

profile of v3, /device:TPU:1, one launch (start us, length us, event | category | flops | bytes accessed | tf_op | source)
XLA Modules:
  0.0 75.5 jit_solution(14887305866483729681)
XLA Ops:
  0.0 73.6 %mixers.1 = bf16[1024,256]{1,0:T(8,128)(2,1)} custom-call(bf16[128,2048]{1,0:T(8,128)(2,1)} %tok.1, bf16[4,32,512]{2,1,0:T(8,128)(2,1)} %pw.1, bf16[1024,128]{1,0:T(8,128)(2,1)} %up.1, bf16[1024,128]{1,0:T(8,128)(2,1)} %dn.1, f32[16,128]{1,0:T(8,128)} %bitcast.4, f32[16,128]{1,0:T(8,128)} %bitcast.5, f32[16,128]{1,0:T(8,128)} %bitcast.6, f32[2,128]{1,0:T(2,128)} %bitcast.7), custom_call_target="tpu_custom_call" | custom-call | tf_op jit(solution)/shard_map/mixers/pallas_call | solution.py:553
  73.6 1.9 %copy.10 = bf16[1024,256]{1,0:T(8,128)(2,1)} copy(bf16[1024,256]{1,0:T(8,128)(2,1)} %mixers.1) | data formatting | bytes 1048576

commit v4 on v3

v4 whole, which is shorter than its diff:
```python
import functools

import jax
import jax.numpy as jnp
from jax import lax
from jax.experimental import pallas as pl
from jax.experimental.pallas import tpu as pltpu
from jax.sharding import PartitionSpec as P

D = 2048
SEQ = 1024
EPS = 1e-06
F32 = jnp.float32
BF16 = jnp.bfloat16
MESH = pl.DeviceIdType.MESH
CH = 256
NCH = SEQ // CH
HALF = SEQ // 2
J = 1
UR = HALF // J


class Phases:
    now = None

    def __call__(self, name):
        if self.now is not None:
            self.now.__exit__(None, None, None)
        self.now = jax.named_scope(name) if name else None
        if name:
            self.now.__enter__()


def kernel(tok, pw, up, dn, pscale_h, gmix_h, gmlp_h, gout_h, out,
           tokv, RL, HX, X, NB, R, RT, PB, UB, DB, PL2, G, SQ, SQ2, H, PART, SS, SB, SO, RH, RY, RZ, ACC,
           pscale, gmix, gmlp, gout, lsem, snd, rcv):
    ph = Phases()
    f = lax.axis_index("fs")
    t = lax.axis_index("tp")
    z, x = f // 4, f % 4
    y, c = t // 2, t % 2

    def fa(d):
        return (1 - c) * (4 * z + (x + d) % 4) + c * (4 * ((z + d) % 4) + x)

    def fb(d):
        return (1 - c) * (4 * ((z + d) % 4) + x) + c * (4 * z + (x + d) % 4)

    pa = (1 - c) * x + c * z
    pb = (1 - c) * z + c * x

    def slot(i, j):
        return 4 * ((pb + j) % 4) + (pa + i) % 4

    def slot_of(g):
        return (1 - c) * g + c * (4 * (g % 4) + g // 4)

    def remote(src, dst, ssem, rsem, fs, tp):
        return pltpu.make_async_remote_copy(
            src_ref=src, dst_ref=dst, send_sem=snd.at[ssem], recv_sem=rcv.at[rsem],
            device_id={"fs": fs, "tp": tp}, device_id_type=MESH)

    def arrived(ref, rsem):
        pltpu.make_async_copy(ref, ref, rcv.at[rsem]).wait()

    sib = 2 * y + 1 - c
    yp = 2 * ((y + 1) % 4) + c
    ym = 2 * ((y + 3) % 4) + c
    own = slot(0, 0)

    ph("a_entry")
    c_tok = pltpu.make_async_copy(tok, tokv, lsem.at[0])
    c_x = pltpu.make_async_copy(
        tok.at[:, pl.ds(pl.multiple_of(256 * t, 256), 256)],
        X.at[pl.ds(pl.multiple_of(128 * t, 128), 128)], lsem.at[1])
    c_u = pltpu.make_async_copy(up, UB.at[own], lsem.at[2])
    c_d = pltpu.make_async_copy(dn, DB.at[own], lsem.at[3])
    c_p = pltpu.make_async_copy(
        pw.at[y, :, pl.ds(pl.multiple_of(256 * c, 256), 256)], PB.at[own], lsem.at[4])
    c_g = [pltpu.make_async_copy(h, v, lsem.at[5 + i])
           for i, (h, v) in enumerate(((pscale_h, pscale), (gmix_h, gmix), (gmlp_h, gmlp), (gout_h, gout)))]
    for cp in [c_tok, c_p, c_u, c_x, c_d] + c_g:
        cp.start()
    barrier = pltpu.get_barrier_semaphore()
    for e in range(1, 8):
        pl.semaphore_signal(barrier, inc=1, device_id={"fs": f, "tp": (t + e) % 8}, device_id_type=MESH)
    for e in (1, 2, 3):
        pl.semaphore_signal(barrier, inc=1, device_id={"fs": fa(e), "tp": t}, device_id_type=MESH)
        pl.semaphore_signal(barrier, inc=1, device_id={"fs": fb(e), "tp": t}, device_id_type=MESH)

    ri = lax.broadcasted_iota(jnp.int32, (128, 128), 0)
    ci = lax.broadcasted_iota(jnp.int32, (128, 128), 1)
    eye = (ri == ci).astype(F32)

    def to_lanes(col):
        return jnp.sum(col * eye, axis=0, keepdims=True)

    def to_column(lanes):
        return jnp.sum(lanes * eye, axis=1, keepdims=True)

    c_tok.wait()
    v = tokv[...].astype(F32)
    r1 = lax.rsqrt(jnp.sum(v * v, axis=1, keepdims=True) / D + EPS)
    R[t] = jnp.broadcast_to(to_lanes(r1), (8, 128))
    c_p.wait()
    c_u.wait()
    c_d.wait()
    pl.semaphore_wait(barrier, 13)

    ph("b_start")
    via = (y + 1 + 2 * c) % 4

    def rows_of(o):
        return pl.ds(pl.multiple_of(128 * o, 128), 128)

    def near(n):
        p = (2 * ((y + (1 if n < 2 else 3)) % 4) + n % 2) if n < 4 else sib
        return remote(tokv.at[:, pl.ds(pl.multiple_of(256 * p, 256), 256)], X.at[rows_of(t)], 0, 0, f, p)

    def relay_out():
        return remote(tokv.at[:, pl.ds(pl.multiple_of(512 * ((y + 2) % 4), 512), 512)], RL, 0, 1, f, 2 * via + c)

    def relay_on(k):
        o = 2 * ((y + 3 + 2 * c) % 4) + c
        return remote(RL.at[:, pl.ds(256 * k, 256)], X.at[rows_of(o)], 0, 19, f, 2 * via + k)

    def edge(k):
        p = 2 * ((y + 2) % 4) + k
        return remote(tokv.at[pl.ds(pl.multiple_of(112 * c, 16), 16), pl.ds(pl.multiple_of(256 * p, 256), 256)],
                      HX.at[c], 0, 20, f, p)

    for k in (0, 1):
        edge(k).start()
    relay_out().start()
    for n in (0, 2, 1, 3, 4):
        near(n).start()

    def r_x(e):
        return remote(R.at[t], R.at[t], 1, 2, f, (t + e) % 8)

    for e in range(1, 8):
        r_x(e).start()

    def p_a(e):
        return remote(PB.at[own], PB.at[own], 1, 3, fa(e), t)

    def p_b(e):
        line = PB.at[pl.ds(4 * pb, 4)]
        return remote(line, line, 1, 4, fb(e), t)

    for e in (1, 3, 2):
        p_a(e).start()

    hrows = (pl.ds(0, HALF), pl.ds(HALF, HALF))
    offs = (0, 3, 1, 2)

    def w_a0(W, s, r, d):
        ref = W.at[own]
        return remote(ref, ref, s, r, fa(1 if d == 0 else 3), t)

    def w_a2(W, s, r, d):
        ref = W.at[slot(3 if d == 0 else 1, 0), hrows[d]]
        return remote(ref, ref, s, r + 1, fa(1 if d == 0 else 3), t)

    def w_b(W, s, r, n, d, h):
        ref = W.at[slot(offs[n], 0)] if h == 2 else W.at[slot(offs[n], 0), hrows[d if h == 0 else 1 - d]]
        return remote(ref, ref, s, r + (10 if h == 1 else 2) + n, fb(1 if d == 0 else 3), t)

    def w_b2(W, s, r, n, d):
        ref = W.at[slot(offs[n], 3 if d == 0 else 1), hrows[d]]
        return remote(ref, ref, s, r + 6 + n, fb(1 if d == 0 else 3), t)

    def pump_a0(W, s, r):
        for d in (0, 1):
            w_a0(W, s, r, d).start()

    def pump_bh(W, s, r, n, h):
        for d in (0, 1):
            w_b(W, s, r, n, d, h).start()

    def pump_b(W, s, r, n):
        pump_bh(W, s, r, n, 0)
        pump_bh(W, s, r, n, 1)

    def pump_bw(W, s, r, n):
        pump_bh(W, s, r, n, 2)

    def pump_a1(W, s, r):
        arrived(W.at[pl.ds(0, 2)], r)
        for d in (0, 1):
            w_a2(W, s, r, d).start()

    def pump_a2(W, s, r):
        arrived(W.at[0], r + 1)

    def pump_b1(W, s, r, n):
        arrived(W.at[0], r + 2 + n)
        for d in (0, 1):
            w_b2(W, s, r, n, d).start()

    def pump_bw1(W, s, r, n):
        arrived(W.at[pl.ds(0, 2)], r + 2 + n)
        for d in (0, 1):
            w_b2(W, s, r, n, d).start()

    def pump_b2(W, s, r, n):
        arrived(W.at[0], r + 6 + n)

    def rest_b(W, s, r, n):
        arrived(W.at[0], r + 10 + n)

    U = (UB, 2, 5)
    V = (DB, 3, 57)
    pump_a0(*U)

    ph("d_wait_pa")
    arrived(PB.at[pl.ds(0, 3)], 3)
    for e in (1, 3, 2):
        p_b(e).start()
    pump_bw(*U, 0)
    ph("d_relay")
    arrived(RL, 1)
    for k in (0, 1):
        relay_on(k).start()
    ph("e_Ua1")
    pump_a1(*U)
    pump_bw(*U, 1)
    pump_bw(*U, 2)
    def row_of(ref):
        return jnp.concatenate([ref[pl.ds(2 * t, 1), :], ref[pl.ds(2 * t + 1, 1), :]], axis=1)

    NB[pl.ds(0, 16), :] = jnp.zeros((16, 256), BF16)
    NB[pl.ds(16 + SEQ, 16), :] = jnp.zeros((16, 256), BF16)
    ph("f_wait_x")
    c_x.wait()
    for cp in c_g:
        cp.wait()
    gm = row_of(gmix)
    arrived(R.at[pl.ds(0, 7)], 2)
    arrived(X.at[pl.ds(0, 640)], 0)
    arrived(HX, 20)
    ph("g_normed")
    order = (0, 1, 3, 2)

    def chunk(p, base=0):
        return (y + base + order[p]) % 4

    def rows_at(q):
        return pl.ds(pl.multiple_of(CH * q, CH), CH)

    def norm_tile(i):
        rc = to_column(R[i, 0:1, :])
        xv = X[rows_of(i), :].astype(F32)
        NB[pl.ds(pl.multiple_of(16 + 128 * i, 16), 128), :] = (xv * rc * gm).astype(BF16)

    for p in range(3):
        for h in (0, 1):
            norm_tile(2 * chunk(p) + h)
    for k in (0, 1):
        i = 2 * chunk(3) + k
        rc = to_column(R[i, 0:1, :])[112 * k:112 * k + 16]
        NB[pl.ds(pl.multiple_of(16 + 128 * i + 112 * k, 16), 16), :] = (HX[k].astype(F32) * rc * gm).astype(BF16)

    reach = 1 + (y >= 1).astype(jnp.int32) + 2 * (y >= 2).astype(jnp.int32) + 4 * (y >= 3).astype(jnp.int32)
    bi = lax.broadcasted_iota(jnp.int32, (128, 160), 0)
    bj = lax.broadcasted_iota(jnp.int32, (128, 160), 1)
    delta = bj - 16 - bi
    band = jnp.where((delta >= -reach) & (delta < reach), 1.0, 0.0).astype(BF16)

    def pl_x(p):
        ref = PL2.at[c, rows_at(chunk(p))]
        return remote(ref, ref, 4, 21 + p, f, sib)

    def pool(p):
        for h in (0, 1):
            i = 2 * chunk(p) + h
            sums = jnp.dot(band, NB[pl.ds(pl.multiple_of(128 * i, 128), 160), :], preferred_element_type=F32)
            pos = 128 * i + lax.broadcasted_iota(jnp.int32, (128, 256), 0)
            count = jnp.minimum(pos + reach, SEQ) - jnp.maximum(pos - reach, 0)
            mine = NB[pl.ds(pl.multiple_of(16 + 128 * i, 16), 128), :].astype(F32)
            PL2[c, rows_of(i), :] = (sums / count.astype(F32) - mine).astype(BF16)
        pl_x(p).start()

    ph("h_pool")
    for p in range(3):
        pool(p)

    ph("i_pb")
    arrived(PB.at[pl.ds(0, 12)], 4)
    ph("j_mix")
    psc = row_of(pscale)
    gml = row_of(gmlp)

    def g_ref(owner, q):
        return G.at[owner, rows_at(q)]

    def g_y(p, d):
        ref = g_ref(t, chunk(p))
        return remote(ref, ref, 5, 25 + p, f, yp if d == 0 else ym)

    def g_sib(k, p):
        owner = (t + (0, 6, 2, 4)[k]) % 8
        q = chunk(p, (0, 3, 1, 2)[k])
        ref = g_ref(owner, q)
        return remote(ref, ref, 5, 31 + q, f, sib)

    def g_fwd(p):
        ref = g_ref(ym if p < 2 else yp, chunk(p, 3 if p < 2 else 1))
        return remote(ref, ref, 5, 29 + p % 2, f, yp if p < 2 else ym)

    pk = [jnp.concatenate([PB[slot_of(8 * k + i)] for i in range(8)], axis=0) for k in (0, 1)]

    def mix(p):
        q = chunk(p)
        rows = rows_at(q)
        arrived(PL2.at[1 - c, rows], 21 + p)
        mixed = (jnp.dot(PL2[0, rows, :], pk[0], preferred_element_type=F32)
                 + jnp.dot(PL2[1, rows, :], pk[1], preferred_element_type=F32)) * psc
        first = (X[rows, :].astype(F32) + mixed).astype(BF16).astype(F32)
        G[t, rows, :] = (first * gml).astype(BF16)
        for d in (0, 1):
            g_y(p, d).start()
        g_sib(0, p).start()
        ACC[0, rows, :] = first[:, :128]
        ACC[1, rows, :] = first[:, 128:]
        sq = jnp.sum(first * first, axis=1, keepdims=True)
        for h in (0, 1):
            SQ[t, pl.ds(2 * q + h, 1), :] = to_lanes(sq[128 * h:128 * h + 128])

    for p in range(3):
        mix(p)
    ph("k_far")
    arrived(X.at[pl.ds(0, 256)], 19)
    for h in (0, 1):
        norm_tile(2 * chunk(3) + h)
    pool(3)
    ph("l_Ub0")
    pump_bw1(*U, 0)
    ph("l_Ua2")
    pump_a2(*U)
    pump_b(*U, 3)
    ph("l_mix3")
    mix(3)
    ph("l_sq")

    def sq_x(e):
        return remote(SQ.at[t], SQ.at[t], 1, 35, f, (t + e) % 8)

    for e in range(1, 8):
        sq_x(e).start()

    def g_pump(p):
        arrived(G.at[0, pl.ds(0, 2 * CH)], 25 + p)
        g_fwd(p).start()
        g_sib(1, p).start()
        g_sib(2, p).start()

    def g_pump2(p):
        arrived(G.at[0, pl.ds(0, 2 * CH)], 29 + p)
        g_sib(3, p).start()
        g_sib(3, p + 2).start()

    ph("m_Ub1")
    pump_bw1(*U, 1)
    ph("m_g0")
    g_pump(0)
    def on(core, *todo):
        @pl.when(c == core)
        def _():
            for fn, args in todo:
                fn(*V, *args)

    ph("m_Ub2")
    pump_bw1(*U, 2)
    pump_a0(*V)
    ph("m_g1")
    g_pump(1)
    ph("m_g2")
    g_pump(2)
    ph("n_Ub3")
    pump_b1(*U, 3)
    on(0, (pump_b, (0,)))
    on(1, (pump_bw, (0,)))
    ph("o_g3")
    g_pump(3)
    ph("o_Va1")
    pump_a1(*V)
    on(0, (pump_bh, (1, 0)))
    on(1, (pump_bw, (1,)), (pump_bw, (2,)))
    ph("o_g20")
    g_pump2(0)
    ph("p_Ub2")
    for n in range(4):
        pump_b2(*U, n)
    rest_b(*U, 3)
    ph("p_g21")
    g_pump2(1)
    ph("p_rt")
    arrived(SQ.at[pl.ds(0, 7)], 35)
    total = SQ[0]
    for i in range(1, 8):
        total = total + SQ[i]
    RT[...] = lax.rsqrt(total / D + EPS)

    def up_rows(q):
        arrived(G.at[pl.ds(0, 4), pl.ds(0, CH)], 31 + q)
        ph(f"t_up{q}")
        rows = pl.ds(CH * q, CH)
        rc = jnp.concatenate([to_column(RT[2 * q + h:2 * q + h + 1, :]) for h in (0, 1)], axis=0)
        lhs = jnp.concatenate([G[i, rows, :] for i in range(8)], axis=1)
        rhs = jnp.concatenate([UB[slot_of(g)] for g in range(16)], axis=1)
        pre = lax.dot_general(lhs, rhs, (((1,), (1,)), ((), ())), preferred_element_type=F32)
        act = jnp.maximum(pre * rc, 0.0)
        H[rows, :] = (act * act).astype(BF16)

    eighth = UR // 2

    def mine(j):
        return pl.ds(pl.multiple_of(HALF * c + UR * j, UR), UR)

    def other(j):
        return pl.ds(pl.multiple_of(HALF * (1 - c) + UR * j, UR), UR)

    qrows = (pl.ds(0, eighth), pl.ds(eighth, eighth))

    def column(k):
        xk = (x + offs[k]) % 4
        return xk, xk // 2

    def c_x2(k, j, d):
        return remote(SS.at[k, j, d], SB.at[k, j, d], 4, 36 + 2 * (J * k + j) + (d != 2), f, sib)

    def y_half(k, j, d):
        return remote(SO.at[k, j, 2, qrows[d]], RH.at[k, j, d], 6, 44 + k + 4 * j, f, yp if d == 0 else ym)

    def y_part(k, j, d, h):
        to = 2 * ((y + 1 + 2 * d) % 4) + column(k)[1]
        rows = pl.ds(pl.multiple_of(HALF * c + UR * j + eighth * h, eighth), eighth)
        return remote(SO.at[k, j, 1 + 2 * d, qrows[h]], RY.at[k, d, rows], 6, 48 + k, f, to)

    def z_x(k, j):
        return remote(SO.at[k, j, 0], RZ.at[k, pl.ds(UR * j, UR)], 4, 52 + k, f, sib)

    def pump(n):
        if n == 0:
            on(0, (pump_b1, (0,)), (pump_bh, (1, 1)), (pump_bh, (2, 0)))
        if n == 1:
            on(0, (pump_b1, (1,)), (pump_bh, (2, 1)), (pump_bh, (3, 0)))
            on(1, (pump_bw1, (0,)), (pump_bw1, (1,)))
        if n == 2:
            on(0, (pump_b1, (2,)), (pump_bh, (3, 1)))
            on(1, (pump_bw1, (2,)), (pump_bw1, (3,)))
        if n == 3:
            on(0, (pump_b1, (3,)))
        if n == 4:
            pump_a2(*V)
            on(1, (pump_bw, (3,)))

    def ready(k):
        on(0, (rest_b, (k,)), (pump_b2, (k,)))
        if k == 3:
            on(1, *((pump_b2, (n,)) for n in range(4)))

    def down(k):
        xk, _ = column(k)
        rhs = jnp.concatenate([DB[slot_of(4 * ((y + d) % 4) + xk)] for d in range(4)], axis=1)
        for j in range(J):
            part = jnp.dot(H[other(j), :], rhs, preferred_element_type=F32)
            for d in (2, 1, 3, 0):
                SS[k, j, d] = part[:, 128 * d:128 * d + 128].astype(BF16)
                c_x2(k, j, d).start()
        for j in range(J):
            PART[(2 * k + j) % 4] = jnp.dot(H[mine(j), :], rhs, preferred_element_type=F32)

    def both(k, j, d, rows):
        return PART[(2 * k + j) % 4, rows, 128 * d:128 * d + 128] + SB[k, j, d, rows].astype(F32)

    def stage1(k, j):
        arrived(SB.at[k, j, 2], 36 + 2 * (J * k + j))
        for d in (0, 1):
            SO[k, j, 2, qrows[d]] = both(k, j, 2, qrows[d]).astype(BF16)
            y_half(k, j, d).start()
        arrived(SB.at[k, j, pl.ds(0, 3)], 37 + 2 * (J * k + j))
        for d in (0, 1):
            b = 1 + 2 * d
            SO[k, j, b, qrows[1 - d]] = both(k, j, b, qrows[1 - d]).astype(BF16)
            y_part(k, j, d, 1 - d).start()

    def stage2(k, j):
        xk, keeper = column(k)
        arrived(RH.at[k, j], 44 + k + 4 * j)
        for d in (0, 1):
            b = 1 + 2 * d
            SO[k, j, b, qrows[d]] = (both(k, j, b, qrows[d]) + RH[k, j, d].astype(F32)).astype(BF16)
            y_part(k, j, d, d).start()

        @pl.when(keeper == c)
        def _():
            ACC[xk % 2, mine(j)] = ACC[xk % 2, mine(j)] + both(k, j, 0, pl.ds(0, UR))

        @pl.when(keeper != c)
        def _():
            SO[k, j, 0] = both(k, j, 0, pl.ds(0, UR)).astype(BF16)
            z_x(k, j).start()

    def stage3(k):
        xk, keeper = column(k)

        @pl.when(keeper == c)
        def _():
            arrived(RZ.at[k], 52 + k)
            rest = pl.ds(pl.multiple_of(HALF * (1 - c), HALF), HALF)
            ACC[xk % 2, rest] = ACC[xk % 2, rest] + RZ[k].astype(F32)
            arrived(RY.at[k], 48 + k)
            ACC[xk % 2] = ACC[xk % 2] + RY[k, 0].astype(F32) + RY[k, 1].astype(F32)

    plan = ("p0 u0 p4 u2 u1 p1 u3 r0 d0 100 101 p2 r1 "
            "d1 110 111 200 201 p3 r2 d2 120 121 210 211 r3 d3 130 131 "
            "220 221 30 230 231 31 32 33")
    for step in plan.split():
        ph("w_" + step)
        a = [int(v) for v in step[1:]]
        if len(a) == 2 and a[1] >= J:
            continue
        {"u": up_rows, "p": pump, "r": ready, "d": down, "1": stage1, "2": stage2, "3": stage3}[step[0]](*a)

    ph("y_sq2")
    for i in range(8):
        rows = pl.ds(128 * i, 128)
        a0, a1 = ACC[0, rows, :], ACC[1, rows, :]
        SQ2[t, pl.ds(i, 1), :] = to_lanes(jnp.sum(a0 * a0 + a1 * a1, axis=1, keepdims=True))

    def t_x(e):
        return remote(SQ2.at[t], SQ2.at[t], 1, 56, f, (t + e) % 8)

    for e in range(1, 8):
        t_x(e).start()
    ph("y_wait")
    arrived(SQ2.at[pl.ds(0, 7)], 56)
    total = SQ2[0]
    for i in range(1, 8):
        total = total + SQ2[i]
    rl = lax.rsqrt(total / D + EPS)

    def out_x(q):
        rows = pl.ds(CH * q, CH)
        return pltpu.make_async_copy(X.at[rows], out.at[rows], lsem.at[q])

    for i in range(8):
        rows = pl.ds(128 * i, 128)
        rc = to_column(rl[i:i + 1, :])
        for h in (0, 1):
            X[rows, 128 * h:128 * h + 128] = (ACC[h, rows, :] * rc * gout[h:h + 1, :]).astype(BF16)
        if i % 2 == 1:
            out_x(i // 2).start()

    ph("z_sent")
    relay_out().wait_send()
    for k in (0, 1):
        relay_on(k).wait_send()
        edge(k).wait_send()
    for n in range(5):
        near(n).wait_send()
    for e in range(1, 8):
        r_x(e).wait_send()
        sq_x(e).wait_send()
        t_x(e).wait_send()
    for e in (1, 2, 3):
        p_a(e).wait_send()
        p_b(e).wait_send()
    for W in (U, V):
        for d in (0, 1):
            w_a0(*W, d).wait_send()
            w_a2(*W, d).wait_send()
            for n in range(4):
                w_b(*W, n, d, 2).wait_send()
                w_b2(*W, n, d).wait_send()
    for q in range(NCH):
        pl_x(q).wait_send()
        g_y(q, 0).wait_send()
        g_y(q, 1).wait_send()
        g_fwd(q).wait_send()
        for k in range(4):
            g_sib(k, q).wait_send()
    for k in range(4):
        for j in range(J):
            for d in range(4):
                c_x2(k, j, d).wait_send()
            for d in (0, 1):
                y_half(k, j, d).wait_send()
                y_part(k, j, d, 0).wait_send()
                y_part(k, j, d, 1).wait_send()

        @pl.when(column(k)[1] != c)
        def _():
            for j in range(J):
                z_x(k, j).wait_send()

    for q in range(NCH):
        out_x(q).wait()
    ph(None)


def local(tokens, pool_weight, pool_scale, gain_mix, gain_mlp, w_up, w_down, gain_out):
    dma = pltpu.SemaphoreType.DMA
    hbm = pl.BlockSpec(memory_space=pltpu.HBM)
    return pl.pallas_call(
        kernel,
        out_shape=jax.ShapeDtypeStruct((SEQ, 256), BF16),
        in_specs=[hbm] * 8,
        out_specs=hbm,
        scratch_shapes=[
            pltpu.VMEM((128, D), BF16),
            pltpu.VMEM((128, 512), BF16),
            pltpu.VMEM((2, 16, 256), BF16),
            pltpu.VMEM((SEQ, 256), BF16),
            pltpu.VMEM((SEQ + 32, 256), BF16),
            pltpu.VMEM((8, 8, 128), F32),
            pltpu.VMEM((8, 128), F32),
            pltpu.VMEM((16, 32, 256), BF16),
            pltpu.VMEM((16, 1024, 128), BF16),
            pltpu.VMEM((16, 1024, 128), BF16),
            pltpu.VMEM((2, SEQ, 256), BF16),
            pltpu.VMEM((8, SEQ, 256), BF16),
            pltpu.VMEM((8, 8, 128), F32),
            pltpu.VMEM((8, 8, 128), F32),
            pltpu.VMEM((SEQ, 1024), BF16),
            pltpu.VMEM((4, UR, 512), F32),
            pltpu.VMEM((4, J, 4, UR, 128), BF16),
            pltpu.VMEM((4, J, 4, UR, 128), BF16),
            pltpu.VMEM((4, J, 4, UR, 128), BF16),
            pltpu.VMEM((4, J, 2, UR // 2, 128), BF16),
            pltpu.VMEM((4, 2, SEQ, 128), BF16),
            pltpu.VMEM((4, HALF, 128), BF16),
            pltpu.VMEM((2, SEQ, 128), F32),
            pltpu.VMEM((16, 128), F32),
            pltpu.VMEM((16, 128), F32),
            pltpu.VMEM((16, 128), F32),
            pltpu.VMEM((2, 128), F32),
            dma((9,)),
            dma((7,)),
            dma((71,)),
        ],
        compiler_params=pltpu.CompilerParams(
            collective_id=0, has_side_effects=True, vmem_limit_bytes=60 * 1024 * 1024),
        name="mixers",
    )(tokens, pool_weight, w_up, w_down, pool_scale.reshape(16, 128), gain_mix.reshape(16, 128),
      gain_mlp.reshape(16, 128), gain_out.reshape(2, 128))


def solution(mesh):
    placed = (P(("fs", "tp"), None), P(None, "fs", None), P(), P(), P(), P("tp", "fs"), P("tp", "fs"), P("tp"))
    return jax.shard_map(local, mesh=mesh, in_specs=placed, out_specs=P("fs", "tp"), check_vma=False)
```

time: 75.7 us -> 73.8 us (0.975)
  Pallas kernels: 73.6 us -> 71.7 us
    pallas_call x1, Pallas kernels: 73.6 us -> 71.7 us  [local(): pl.pallas_call(kernel, out_shape=jax.ShapeDtypeStruct((SEQ, 256), BF16),...]
where the time goes in v4:
time: 73.8 us; the launch traced here: 73.6 us
  Pallas kernels  71.7 us (97%)
  local copies, waits for them, and re-layouts  1.87 us (3%)
    pallas_call x1, Pallas kernels, local(): pl.pallas_call(kernel, out_shape=jax.ShapeDtypeStruct((SEQ, 256), BF16),...  71.7 us
    unnamed x1, local copies, waits for them, and re-layouts  1.87 us

profile of v4, /device:TPU:1, one launch (start us, length us, event | category | flops | bytes accessed | tf_op | source)
XLA Modules:
  0.0 73.6 jit_solution(4422779368699549670)
XLA Ops:
  0.0 71.7 %mixers.1 = bf16[1024,256]{1,0:T(8,128)(2,1)} custom-call(bf16[128,2048]{1,0:T(8,128)(2,1)} %tok.1, bf16[4,32,512]{2,1,0:T(8,128)(2,1)} %pw.1, bf16[1024,128]{1,0:T(8,128)(2,1)} %up.1, bf16[1024,128]{1,0:T(8,128)(2,1)} %dn.1, f32[16,128]{1,0:T(8,128)} %bitcast.4, f32[16,128]{1,0:T(8,128)} %bitcast.5, f32[16,128]{1,0:T(8,128)} %bitcast.6, f32[2,128]{1,0:T(2,128)} %bitcast.7), custom_call_target="tpu_custom_call" | custom-call | tf_op jit(solution)/shard_map/mixers/pallas_call | solution.py:607
  71.8 1.9 %copy.10 = bf16[1024,256]{1,0:T(8,128)(2,1)} copy(bf16[1024,256]{1,0:T(8,128)(2,1)} %mixers.1) | data formatting | bytes 1048576

commit v5 on v4

--- a/solution.py
+++ b/solution.py
@@ -389,12 +389,12 @@
     on(1, (pump_bw, (1,)), (pump_bw, (2,)))
     ph("o_g20")
     g_pump2(0)
+    ph("p_g21")
+    g_pump2(1)
     ph("p_Ub2")
     for n in range(4):
         pump_b2(*U, n)
     rest_b(*U, 3)
-    ph("p_g21")
-    g_pump2(1)
     ph("p_rt")
     arrived(SQ.at[pl.ds(0, 7)], 35)
     total = SQ[0]
@@ -514,15 +514,16 @@
             arrived(RY.at[k], 48 + k)
             ACC[xk % 2] = ACC[xk % 2] + RY[k, 0].astype(F32) + RY[k, 1].astype(F32)
 
-    plan = ("p0 u0 p4 u2 u1 p1 u3 r0 d0 100 101 p2 r1 "
-            "d1 110 111 200 201 p3 r2 d2 120 121 210 211 r3 d3 130 131 "
-            "220 221 30 230 231 31 32 33")
-    for step in plan.split():
-        ph("w_" + step)
-        a = [int(v) for v in step[1:]]
-        if len(a) == 2 and a[1] >= J:
-            continue
-        {"u": up_rows, "p": pump, "r": ready, "d": down, "1": stage1, "2": stage2, "3": stage3}[step[0]](*a)
+    plan = (
+        (pump, 0), (up_rows, 0), (pump, 4), (up_rows, 2), (up_rows, 1), (pump, 1),
+        (up_rows, 3), (ready, 0), (down, 0), (stage1, 0, 0), (pump, 2), (ready, 1),
+        (down, 1), (stage1, 1, 0), (stage2, 0, 0), (pump, 3), (ready, 2), (down, 2),
+        (stage1, 2, 0), (stage2, 1, 0), (ready, 3), (down, 3), (stage1, 3, 0), (stage2, 2, 0),
+        (stage3, 0), (stage2, 3, 0), (stage3, 1), (stage3, 2), (stage3, 3),
+    )
+    for step, *which in plan:
+        ph("w_" + step.__name__ + str(which[0]))
+        step(*which)
 
     ph("y_sq2")
     for i in range(8):

time: 73.8 us -> 73.8 us (level)
  no operation moved by 1% of the time
where the time goes in v5:
time: 73.8 us; the launch traced here: 73.6 us
  Pallas kernels  71.7 us (97%)
  local copies, waits for them, and re-layouts  1.87 us (3%)
    pallas_call x1, Pallas kernels, local(): pl.pallas_call(kernel, out_shape=jax.ShapeDtypeStruct((SEQ, 256), BF16),...  71.7 us
    unnamed x1, local copies, waits for them, and re-layouts  1.87 us

profile of v5, /device:TPU:1, one launch (start us, length us, event | category | flops | bytes accessed | tf_op | source)
XLA Modules:
  0.0 73.6 jit_solution(6720577483613833810)
XLA Ops:
  0.0 71.7 %mixers.1 = bf16[1024,256]{1,0:T(8,128)(2,1)} custom-call(bf16[128,2048]{1,0:T(8,128)(2,1)} %tok.1, bf16[4,32,512]{2,1,0:T(8,128)(2,1)} %pw.1, bf16[1024,128]{1,0:T(8,128)(2,1)} %up.1, bf16[1024,128]{1,0:T(8,128)(2,1)} %dn.1, f32[16,128]{1,0:T(8,128)} %bitcast.4, f32[16,128]{1,0:T(8,128)} %bitcast.5, f32[16,128]{1,0:T(8,128)} %bitcast.6, f32[2,128]{1,0:T(2,128)} %bitcast.7), custom_call_target="tpu_custom_call" | custom-call | tf_op jit(solution)/shard_map/mixers/pallas_call | solution.py:608
  71.8 1.9 %copy.10 = bf16[1024,256]{1,0:T(8,128)(2,1)} copy(bf16[1024,256]{1,0:T(8,128)(2,1)} %mixers.1) | data formatting | bytes 1048576

commit v6 on v5

--- a/solution.py
+++ b/solution.py
@@ -521,15 +521,20 @@
         (stage1, 2, 0), (stage2, 1, 0), (ready, 3), (down, 3), (stage1, 3, 0), (stage2, 2, 0),
         (stage3, 0), (stage2, 3, 0), (stage3, 1), (stage3, 2), (stage3, 3),
     )
+    last = column(3)[0] % 2
+
+    def squares(half):
+        return [to_lanes(jnp.sum(ACC[half, pl.ds(128 * i, 128), :] * ACC[half, pl.ds(128 * i, 128), :],
+                                 axis=1, keepdims=True)) for i in range(8)]
+
     for step, *which in plan:
+        if step is stage3 and which[0] == 3:
+            SQ2[t] = jnp.concatenate(squares(1 - last), axis=0)
         ph("w_" + step.__name__ + str(which[0]))
         step(*which)
 
     ph("y_sq2")
-    for i in range(8):
-        rows = pl.ds(128 * i, 128)
-        a0, a1 = ACC[0, rows, :], ACC[1, rows, :]
-        SQ2[t, pl.ds(i, 1), :] = to_lanes(jnp.sum(a0 * a0 + a1 * a1, axis=1, keepdims=True))
+    SQ2[t] = SQ2[t] + jnp.concatenate(squares(last), axis=0)
 
     def t_x(e):
         return remote(SQ2.at[t], SQ2.at[t], 1, 56, f, (t + e) % 8)

time: 73.8 us -> 73.8 us (level)
  no operation moved by 1% of the time
where the time goes in v6:
time: 73.8 us; the launch traced here: 73.6 us
  Pallas kernels  71.7 us (97%)
  local copies, waits for them, and re-layouts  1.87 us (3%)
    pallas_call x1, Pallas kernels, local(): pl.pallas_call(kernel, out_shape=jax.ShapeDtypeStruct((SEQ, 256), BF16),...  71.7 us
    unnamed x1, local copies, waits for them, and re-layouts  1.87 us

profile of v6, /device:TPU:1, one launch (start us, length us, event | category | flops | bytes accessed | tf_op | source)
XLA Modules:
  0.0 73.6 jit_solution(10739112684253228662)
XLA Ops:
  0.0 71.7 %mixers.1 = bf16[1024,256]{1,0:T(8,128)(2,1)} custom-call(bf16[128,2048]{1,0:T(8,128)(2,1)} %tok.1, bf16[4,32,512]{2,1,0:T(8,128)(2,1)} %pw.1, bf16[1024,128]{1,0:T(8,128)(2,1)} %up.1, bf16[1024,128]{1,0:T(8,128)(2,1)} %dn.1, f32[16,128]{1,0:T(8,128)} %bitcast.4, f32[16,128]{1,0:T(8,128)} %bitcast.5, f32[16,128]{1,0:T(8,128)} %bitcast.6, f32[2,128]{1,0:T(2,128)} %bitcast.7), custom_call_target="tpu_custom_call" | custom-call | tf_op jit(solution)/shard_map/mixers/pallas_call | solution.py:613
  71.8 1.9 %copy.10 = bf16[1024,256]{1,0:T(8,128)(2,1)} copy(bf16[1024,256]{1,0:T(8,128)(2,1)} %mixers.1) | data formatting | bytes 1048576
